TPU v7x, 256 devices: a whole 4x4x8 slice. The times are simulated.
256 devices in a mesh: ep: 128 (over z, y, x), tp: 2 (over core).
Axes of the slice: x: 4, y: 4, z: 8, core: 2. Of those that a mesh axis runs over, the one named last changes fastest.
Arguments:
- residual_in: bfloat16 [2048, 1024], P('ep'), may hold values from -6 to 6
- lengths: int32 [2048], P('ep'), may hold values from 64 to 1024
- cache_keys: bfloat16 [2048, 2, 1024, 128], P('ep', 'tp'), may hold values from -7 to 7
- cache_values: bfloat16 [2048, 2, 1024, 128], P('ep', 'tp'), may hold values from -6 to 6
- attend_gain: bfloat16 [1024], replicated, may hold values from 0.099609375 to 1.8984375
- query_proj: bfloat16 [1024, 512], P(None, 'tp'), may hold values from -0.1875 to 0.1875
- key_proj: bfloat16 [1024, 256], P(None, 'tp'), may hold values from -0.1875 to 0.1875
- value_proj: bfloat16 [1024, 256], P(None, 'tp'), may hold values from -0.1875 to 0.1875
- lambdas: float32 [4], P('tp'), may hold values from 0.3 to 0.8
- head_gain: bfloat16 [128], replicated, may hold values from 0.099609375 to 1.8984375
- out_proj: bfloat16 [512, 1024], P('tp'), may hold values from -0.25 to 0.25
- channel_gain: bfloat16 [1024], replicated, may hold values from 0.099609375 to 1.8984375
- routes: int32 [2048, 6], P('ep'), may hold values from 0 to 127, all different within a row; in each aligned block of 16 rows (0 to 15, 16 to 31, ...) at most 2 rows name the same one
- route_weight: float32 [2048, 6], P('ep'), may hold values from 0.1 to 1
- expert_gate: bfloat16 [128, 1024, 512], P('ep', None, 'tp'), may hold values from -0.1875 to 0.1875
- expert_up: bfloat16 [128, 1024, 512], P('ep', None, 'tp'), may hold values from -0.1875 to 0.1875
- expert_down: bfloat16 [128, 512, 1024], P('ep', 'tp'), may hold values from -0.25 to 0.25
- dense_gate: bfloat16 [1024, 4096], P(None, ('ep', 'tp')), may hold values from -0.1875 to 0.1875
- dense_up: bfloat16 [1024, 4096], P(None, ('ep', 'tp')), may hold values from -0.1875 to 0.1875
- dense_down: bfloat16 [4096, 1024], P(('ep', 'tp')), may hold values from -0.09375 to 0.09375
- dense_mixer: bfloat16 [1024], replicated, may hold values from -0.1875 to 0.1875
Outputs:
- residual_out: bfloat16 [2048, 1024], P('ep')
- new_keys: bfloat16 [2048, 2, 128], P('ep', 'tp')
- new_values: bfloat16 [2048, 2, 128], P('ep', 'tp')
Inputs may be any that keep to these rules, and one draw needn't show every extreme that they name: `routes`: each row names 6 different experts; in each aligned block of 16 rows (the rows of one index of ep) no expert is named by more than 2 rows, and in some blocks one expert is named by exactly 2 rows.
All inputs are finite; a program needn't handle non-finite values.
Results may differ from a plain program's by a relative error of at most 0.015.
Values may be sent and summed in bfloat16 or wider, within the bound.
A program may use at most 64 MiB of HBM per device.

v0:
```python
import functools

import jax
import jax.numpy as jnp
from jax import lax
from jax.sharding import Mesh
from jax.sharding import PartitionSpec as P

HEAD = 64
EP = ("ep_0", "ep_1", "ep_2")
EP_TP = ("ep_0", "ep_1", "ep_2", "tp")


NORM_EPSILON = 1e-06
ROTARY_BASE = 10000.0
HEAD_SCALE = 0.8


def cut_along(shard, dim, count):
    shape = shard.shape
    blocks = shard.reshape(*shape[:dim], count, shape[dim] // count, *shape[dim + 1 :])
    return jnp.moveaxis(blocks, dim, 0)


def sum_at_owner(shard, axis, dim):
    count = lax.axis_size(axis)
    blocks = lax.all_to_all(cut_along(shard, dim, count), axis, 0, 0, tiled=True)
    return jnp.sum(blocks.astype(jnp.float32), axis=0)


def sent_to_all(shard, axis):
    copies = jnp.broadcast_to(shard, (lax.axis_size(axis), *shard.shape))
    return lax.all_to_all(copies, axis, split_axis=0, concat_axis=0, tiled=True)


def of_everyone(shard, axis):
    everything = sent_to_all(shard, axis)
    return jnp.sum(everything.astype(jnp.float32), axis=0)


def in_order(blocks, dim):
    shape = list(blocks.shape[1:])
    shape[dim] *= blocks.shape[0]
    return jnp.moveaxis(blocks, 0, dim).reshape(shape)


def collect(shard, axis, dim):
    return in_order(sent_to_all(shard, axis), dim)


def gather_turned(arrays, axis, dims):
    turned = [jnp.moveaxis(a, dim, 0) for a, dim in zip(arrays, dims)]
    both = jnp.concatenate([t.reshape(len(t), -1) for t in turned], axis=1)
    out, at, done = (lax.all_gather(both, axis, axis=0, tiled=True), 0, [])
    for t, dim in zip(turned, dims):
        share = out[:, at : at + t[0].size].reshape(-1, *t.shape[1:])
        done.append(jnp.moveaxis(share, 0, dim))
        at += t[0].size
    return tuple(done)


def whole_of(shard, axes, dim):
    if not axes:
        return shard
    nearer = lax.all_gather(shard, axes[-1], axis=dim, tiled=True)
    return whole_of(nearer, axes[:-1], dim)


def summed_rows(shard, axes, dim):
    if not axes:
        return shard
    nearer = lax.psum_scatter(shard, axes[0], scatter_dimension=dim, tiled=True)
    return summed_rows(nearer, axes[1:], dim)


def norm_scale(vectors, gain_vector):
    mean_square = jnp.mean(vectors * vectors, axis=-1, keepdims=True)
    return vectors * lax.rsqrt(mean_square + NORM_EPSILON) * gain_vector


def rotate(vectors, position):
    half_width = vectors.shape[-1] // 2
    inverse = ROTARY_BASE ** (-jnp.arange(half_width, dtype=jnp.float32) / half_width)
    angles = position[..., None] * inverse
    cosine = jnp.cos(angles)
    sine_part = jnp.sin(angles)
    front_half = vectors[..., :half_width]
    back_half = vectors[..., half_width:]
    return jnp.concatenate(
        [front_half * cosine - back_half * sine_part, back_half * cosine + front_half * sine_part],
        axis=-1,
    )


def slot_layout(routes, route_weight, experts_all, capacity):
    sequences, route_count = routes.shape
    pair_count = sequences * route_count
    chosen = routes.reshape(pair_count)
    onehot = (
        chosen[:, None] == lax.broadcasted_iota(jnp.int32, (pair_count, experts_all), 1)
    ).astype(jnp.int32)
    slot_index = jnp.sum((jnp.cumsum(onehot, axis=0) - onehot) * onehot, axis=1)
    placement = chosen * capacity + slot_index
    slot_match = (
        placement[:, None]
        == lax.broadcasted_iota(jnp.int32, (pair_count, experts_all * capacity), 1)
    ).astype(jnp.float32)
    weighted = slot_match * route_weight.reshape(pair_count, 1)
    combine_rows = jnp.sum(weighted.reshape(sequences, route_count, experts_all * capacity), axis=1)
    return (slot_match.astype(jnp.bfloat16), combine_rows)


def serve_slots(expert_weights, arrived):
    gate_weight, up_weight, down_weight = expert_weights
    sources, count, model_width = arrived.shape
    row_block = arrived.reshape(sources * count, model_width)
    gated = jnp.dot(row_block, gate_weight, preferred_element_type=jnp.float32)
    upper = jnp.dot(row_block, up_weight, preferred_element_type=jnp.float32)
    hidden = (jax.nn.silu(gated) * upper).astype(jnp.bfloat16)
    partial_value = jnp.dot(hidden, down_weight, preferred_element_type=jnp.float32)
    halved = sum_at_owner(partial_value.astype(jnp.bfloat16), "tp", 1).astype(jnp.bfloat16)
    halved = halved.reshape(sources, count, halved.shape[1])
    return lax.all_to_all(halved, EP, split_axis=0, concat_axis=0, tiled=True)


def dense_rows(weights, mixer, piece):
    gate_weight, up_weight, down_weight = weights
    switch = jax.nn.sigmoid(jnp.dot(piece, mixer, preferred_element_type=jnp.float32))
    gated = jnp.dot(piece, gate_weight, preferred_element_type=jnp.float32)
    upper = jnp.dot(piece, up_weight, preferred_element_type=jnp.float32)
    hidden = (jax.nn.silu(gated) * upper).astype(jnp.bfloat16)
    return switch[:, None] * jnp.dot(hidden, down_weight, preferred_element_type=jnp.float32)


def per_device(
    residual_in,
    lengths,
    cache_keys,
    cache_values,
    attend_gain,
    query_proj,
    key_proj,
    value_proj,
    lambdas,
    head_gain,
    out_proj,
    channel_gain,
    routes,
    route_weight,
    expert_gate,
    expert_up,
    expert_down,
    dense_gate,
    dense_up,
    dense_down,
    dense_mixer,
):
    sequences, model_width = residual_in.shape
    kv_local = cache_keys.shape[1]
    cache_length = cache_keys.shape[2]
    value_width = cache_values.shape[3]
    heads_local = lambdas.shape[0]
    group_size = heads_local // kv_local
    residual = residual_in.astype(jnp.float32)
    normed = norm_scale(residual, attend_gain.astype(jnp.float32)).astype(jnp.bfloat16)
    queries = jnp.dot(normed, query_proj, preferred_element_type=jnp.float32).reshape(
        sequences, heads_local, 2, HEAD
    )
    key_rows = jnp.dot(normed, key_proj, preferred_element_type=jnp.float32).reshape(
        sequences, kv_local, 2, HEAD
    )
    new_values = (
        jnp.dot(normed, value_proj, preferred_element_type=jnp.float32)
        .astype(jnp.bfloat16)
        .reshape(sequences, kv_local, value_width)
    )
    position = lengths.astype(jnp.float32)[:, None, None]
    queries = (
        rotate(queries, position)
        .astype(jnp.bfloat16)
        .reshape(sequences, kv_local, group_size, 2, HEAD)
    )
    new_keys = rotate(key_rows, position).astype(jnp.bfloat16)
    cached = cache_keys.reshape(sequences, kv_local, cache_length, 2, HEAD)
    score_scale = HEAD ** (-0.5)
    scores = (
        jnp.einsum("sagmd,salmd->sagml", queries, cached, preferred_element_type=jnp.float32)
        * score_scale
    )
    own_score = (
        jnp.einsum("sagmd,samd->sagm", queries, new_keys, preferred_element_type=jnp.float32)
        * score_scale
    )
    visible = (lax.broadcasted_iota(jnp.int32, (sequences, cache_length), 1) < lengths[:, None])[
        :, None, None, None, :
    ]
    exponent = jnp.where(visible, jnp.exp(scores), 0.0)
    own_exponent = jnp.exp(own_score)
    denominator = jnp.sum(exponent, axis=-1) + own_exponent
    probability = exponent / denominator[..., None]
    own_probability = own_exponent / denominator
    mixing = lambdas.reshape(kv_local, group_size)[None, :, :, None]
    weight = (probability[..., 0, :] - mixing * probability[..., 1, :]).astype(jnp.bfloat16)
    own_weight = (own_probability[..., 0] - mixing[..., 0] * own_probability[..., 1]).astype(
        jnp.bfloat16
    )
    attended = jnp.einsum(
        "sagl,sale->sage", weight, cache_values, preferred_element_type=jnp.float32
    )
    attended = (
        attended
        + own_weight.astype(jnp.float32)[..., None] * new_values.astype(jnp.float32)[:, :, None, :]
    )
    head_rows = (
        (norm_scale(attended, head_gain.astype(jnp.float32)) * HEAD_SCALE)
        .astype(jnp.bfloat16)
        .reshape(sequences, heads_local * value_width)
    )
    partial_value = jnp.dot(head_rows, out_proj, preferred_element_type=jnp.float32)
    attend_out = of_everyone(partial_value.astype(jnp.bfloat16), "tp").astype(jnp.float32)
    middle = (residual + attend_out).astype(jnp.bfloat16)
    normed_second = norm_scale(middle.astype(jnp.float32), channel_gain.astype(jnp.float32)).astype(
        jnp.bfloat16
    )
    experts_all = lax.axis_size(EP)
    route_count = routes.shape[1]
    capacity = (sequences * route_count + experts_all - 1) // experts_all * 2
    slot_match, combine_rows = slot_layout(routes, route_weight, experts_all, capacity)
    repeated = jnp.repeat(normed_second, route_count, axis=0)
    outgoing = lax.dot_general(
        slot_match, repeated, (((0,), (0,)), ((), ())), preferred_element_type=jnp.float32
    )
    outgoing = outgoing.astype(jnp.bfloat16).reshape(experts_all, capacity, model_width)
    serve = functools.partial(serve_slots, (expert_gate[0], expert_up[0], expert_down[0]))
    returned = serve(lax.all_to_all(outgoing, EP, split_axis=0, concat_axis=0, tiled=True))
    returned = returned.reshape(experts_all * capacity, returned.shape[2]).astype(jnp.float32)
    routed_half = jnp.dot(combine_rows, returned, precision=lax.Precision.HIGHEST)
    routed = collect(routed_half.astype(jnp.bfloat16), "tp", 1).astype(routed_half.dtype)
    gathered = gather_turned((dense_gate, dense_up, dense_down), "tp", (1, 1, 0))
    row_share = sequences // lax.axis_size("tp")
    own_rows = lax.dynamic_slice_in_dim(
        normed_second, lax.axis_index("tp") * row_share, row_share, 0
    )
    dense_terms = dense_rows(gathered, dense_mixer, whole_of(own_rows, EP, 0))
    summed = summed_rows(dense_terms.astype(jnp.bfloat16), EP, 0).astype(jnp.float32)
    dense_out = collect(summed.astype(jnp.bfloat16), "tp", 0).astype(summed.dtype)
    residual_out = (middle.astype(jnp.float32) + routed + dense_out).astype(jnp.bfloat16)
    return (residual_out, new_keys.reshape(sequences, kv_local, 2 * HEAD), new_values)


def solution(mesh):
    finer = Mesh(mesh.devices.reshape(8, 4, 4, mesh.shape["tp"]), ("ep_0", "ep_1", "ep_2", "tp"))
    placed = (
        P(EP, None),
        P(EP),
        P(EP, "tp", None, None),
        P(EP, "tp", None, None),
        P(),
        P(None, "tp"),
        P(None, "tp"),
        P(None, "tp"),
        P("tp"),
        P(),
        P("tp", None),
        P(),
        P(EP, None),
        P(EP, None),
        P(EP, None, "tp"),
        P(EP, None, "tp"),
        P(EP, "tp", None),
        P(None, EP_TP),
        P(None, EP_TP),
        P(EP_TP, None),
        P(),
    )
    return jax.shard_map(
        per_device,
        mesh=finer,
        in_specs=placed,
        out_specs=(P(EP, None), P(EP, "tp", None), P(EP, "tp", None)),
        check_vma=False,
    )
```

profile of v0, /device:TPU:1, one launch (start us, length us, event | category | flops | bytes accessed | tf_op | source)
XLA Modules:
  0.0 221.9 jit_solution(1946623105309924847)
XLA Ops:
  7.2 0.7 convert_element_type.132
  7.9 0.7 iota_compare_fusion.2
  8.6 0.7 convert_element_type.130
  9.3 0.9 fusion.31
  10.2 1.2 fusion.59
  11.5 1.3 fusion.61
  12.8 0.1 reshape.276
  12.9 0.1 fusion.64
  13.0 0.1 multiply_cosine_fusion
  13.1 0.1 subtract_convert_fusion.1
  13.2 0.1 maximum_bitcast_fusion
  13.3 0.2 fusion.48
  13.5 0.1 copy.95
  13.7 6.4 %copy.84 = bf16[16,1,1024,128]{2,3,0,1:T(8,128)(2,1)} copy(bf16[16,1,1024,128]{3,2,1,0:T(8,128)(2,1)} %param.23) | data formatting | bytes 8388608 | tf_op args[2]
  20.1 3.1 %fusion.65 = (f32[16,2,2]{1,2,0:T(2,128)S(1)}, f32[16,1,2,2,1024]{4,2,3,0,1:T(2,128)S(1)}) fusion(bf16[16,1024,2,64]{1,3,2,0:T(8,128)(2,1)} %bitcast.114, bf16[16,2,2,32]{3,1,2,0:T(2,128)(2,1)S(1)} %get-tuple-element.6, bf16[16,2,2,32]{3,1,2,0:T(2,128)(2,1)S(1)} %get-tuple-element.5, pred[16,1024]{1,0:T(8,128)(4,1)S(1)} %iota_compare_fusion.2), kind=kOutput, calls=%fused_computation.109 | convolution fusion | flops 8601536 | bytes 4481280 | tf_op jit(solution)/shard_map/sagmd,salmd->sagml/dot_general | solution.py:187
  23.1 0.1 copy.85
  23.2 0.1 copy.87
  23.4 0.1 copy.89
  23.5 0.8 fusion.66
  24.3 0.2 broadcast_divide_fusion
  24.6 3.0 %multiply_reduce_fusion = (f32[16,2]{1,0:T(8,128)S(1)}, f32[16,2,128]{2,1,0:T(2,128)S(1)}) fusion(f32[16,128]{1,0:T(8,128)S(1)} %get-tuple-element.17, f32[16,2]{1,0:T(8,128)S(1)} %copy.89, bf16[16,1,1024,128]{3,2,1,0:T(8,128)(2,1)} %param.24, f32[16,1,2,2,1024]{4,2,3,0,1:T(2,128)S(1)} %broadcast_divide_fusion, f32[2]{0:T(128)S(1)} %copy-done.10), kind=kOutput, calls=%fused_computation.76 | convolution fusion | flops 8503264 | bytes 4481288 | tf_op jit(solution)/shard_map/sagl,sale->sage/dot_general | solution.py:207
  27.6 0.1 multiply_convert_fusion.1
  27.7 0.2 convolution_convert_fusion.2
  27.9 0.6 broadcast_in_dim.22
  28.6 6.5 %all-to-all-start = ((bf16[2,16,1024]{2,1,0:T(8,128)(2,1)}), bf16[2,16,1024]{2,1,0:T(8,128)(2,1)S(1)}, u32[]{:S(2)}, u32[]{:S(2)}) async-start(bf16[2,16,1024]{2,1,0:T(8,128)(2,1)} %broadcast_in_dim.22), calls=%async_computation | async-start | bytes 131072 | tf_op jit(solution)/shard_map/all_to_all | solution.py:33
  35.0 1.1 all-to-all-done
  36.1 0.1 fusion.35
  36.4 9.0 %all_gather.12 = bf16[32,1024]{1,0:T(8,128)(2,1)S(1)} all-gather(bf16[8,1024]{1,0:T(8,128)(2,1)S(1)} %constant_dynamic-slice_fusion), channel_id=1, replica_groups=mesh['ep_0'=8,'ep_1'=4,'ep_2'=4,'tp'=2] {'ep_2'}, dimensions={0}, use_global_device_ids=true | all-gather | bytes 81920 | tf_op jit(solution)/shard_map/all_gather | solution.py:65
  45.3 10.1 %all_gather.13 = bf16[128,1024]{1,0:T(8,128)(2,1)} all-gather(bf16[32,1024]{1,0:T(8,128)(2,1)S(1)} %all_gather.12), channel_id=1, replica_groups=mesh['ep_0'=8,'ep_1'=4,'ep_2'=4,'tp'=2] {'ep_1'}, dimensions={0}, use_global_device_ids=true | all-gather | bytes 327680 | tf_op jit(solution)/shard_map/all_gather | solution.py:65
  55.6 7.7 %all_gather.15 = bf16[32,3072]{1,0:T(8,128)(2,1)S(1)} all-gather(bf16[16,3072]{1,0:T(8,128)(2,1)S(1)} %pad_maximum_fusion), channel_id=1, replica_groups=mesh['ep_0'=8,'ep_1'=4,'ep_2'=4,'tp'=2] {'tp'}, dimensions={0}, use_global_device_ids=true | all-gather | bytes 294912 | tf_op jit(solution)/shard_map/all_gather | solution.py:54
  63.3 35.2 %all-gather.2.cloned.1.call-done = bf16[1024,1024]{1,0:T(8,128)(2,1)} async-done(((bf16[128,1024]{1,0:T(8,128)(2,1)}), bf16[1024,1024]{1,0:T(8,128)(2,1)}) %all-gather.2.cloned.1.call-update) | async-done | bytes 2097168 | tf_op jit(solution)/shard_map/all_gather | solution.py:65
  98.6 2.4 %fusion.67 = f32[1,1024]{1,0:T(1,128)S(1)} fusion(bf16[1024,1024]{1,0:T(8,128)(2,1)} %all-gather.2.cloned.1.call-done, bf16[1024,1]{0,1:T(2,128)(2,1)S(1)} %reshape.293), kind=kOutput, calls=%fused_computation.111 | convolution fusion | flops 2097152 | bytes 2103296 | tf_op jit(solution)/shard_map/dot_general | solution.py:128
  101.0 0.7 fusion.43
  101.7 2.7 %multiply_convert_fusion = bf16[1024,1024]{1,0:T(8,128)(2,1)} fusion(f32[1024]{0:T(1024)S(1)} %add_divide_fusion, bf16[1024,1024]{1,0:T(8,128)(2,1)S(1)} %copy-done.1, f32[1024,32]{0,1:T(8,128)S(1)} %fusion.43, bf16[32,3072]{1,0:T(8,128)(2,1)S(1)} %all_gather.15), kind=kOutput, calls=%fused_computation.2 | convolution fusion | flops 136511488 | bytes 4460544 | tf_op jit(solution)/shard_map/dot_general | solution.py:132
  104.5 0.5 copy-done.8
  105.1 0.1 copy.90
  105.2 0.1 eq.23
  105.3 0.1 fusion.47
  105.4 0.1 reduce_window_sum.11
  105.5 0.2 select_reduce_fusion.1
  105.7 0.4 convolution_convert_fusion.1
  106.1 0.2 reshape.282
  106.3 28.9 %all_to_all.30 = bf16[128,2,1024]{2,1,0:T(2,128)(2,1)S(1)} all-to-all(bf16[128,2,1024]{2,1,0:T(2,128)(2,1)S(1)} %reshape.282), channel_id=1, replica_groups=mesh['ep_0'=8,'ep_1'=4,'ep_2'=4,'tp'=2] {'ep_0','ep_1','ep_2'}, dimensions={0} | all-to-all | bytes 1048576 | tf_op jit(solution)/shard_map/all_to_all | solution.py:235
  135.2 0.2 reshape.283
  135.4 0.3 fusion.14
  135.7 0.7 convolution_convert_fusion
  136.5 13.8 %all_to_all.31 = bf16[2,256,512]{2,1,0:T(8,128)(2,1)S(1)} all-to-all(bf16[2,256,512]{2,1,0:T(8,128)(2,1)S(1)} %bitcast.115), channel_id=1, replica_groups=mesh['ep_0'=8,'ep_1'=4,'ep_2'=4,'tp'=2] {'tp'}, dimensions={0} | all-to-all | bytes 1048576 | tf_op jit(solution)/shard_map/all_to_all | solution.py:27
  150.3 0.1 reduce_sum.88
  150.4 0.8 reshape.285
  151.2 6.2 %all-to-all-start.3 = ((bf16[128,2,512]{2,1,0:T(2,128)(2,1)}), bf16[128,2,512]{2,1,0:T(2,128)(2,1)S(1)}, u32[]{:S(2)}, u32[]{:S(2)}) async-start(bf16[128,2,512]{2,1,0:T(2,128)(2,1)} %reshape.285), calls=%async_computation.3 | async-start | bytes 524288 | tf_op jit(solution)/shard_map/all_to_all | solution.py:123
  157.5 0.1 copy.91
  157.6 0.1 pad_maximum_fusion.2
  157.7 0.7 convert_element_type.160
  158.4 0.1 select_reduce_fusion
  158.5 12.8 %all-to-all-done.3 = bf16[128,2,512]{2,1,0:T(2,128)(2,1)S(1)} async-done(((bf16[128,2,512]{2,1,0:T(2,128)(2,1)}), bf16[128,2,512]{2,1,0:T(2,128)(2,1)S(1)}, u32[]{:S(2)}, u32[]{:S(2)}) %all-to-all-start.3) | async-done | bytes 262176 | tf_op jit(solution)/shard_map/all_to_all | solution.py:123
  171.4 0.1 reshape.286
  171.5 0.2 convolution_convert_fusion.3
  171.7 0.6 broadcast_in_dim.24
  172.3 5.4 %all-to-all-start.4 = ((bf16[2,16,512]{2,1,0:T(8,128)(2,1)}), bf16[2,16,512]{2,1,0:T(8,128)(2,1)S(1)}, u32[]{:S(2)}, u32[]{:S(2)}) async-start(bf16[2,16,512]{2,1,0:T(8,128)(2,1)} %broadcast_in_dim.24), calls=%async_computation.4 | async-start | bytes 65536 | tf_op jit(solution)/shard_map/all_to_all | solution.py:33
  177.7 4.8 %reduce-scatter.6.cloned.1.call-done = bf16[32,1024]{1,0:T(8,128)(2,1)} async-done(((bf16[128,1024]{1,0:T(8,128)(2,1)}), bf16[32,1024]{1,0:T(8,128)(2,1)}) %reduce-scatter.6.cloned.1.call-update) | async-done | bytes 65552 | tf_op jit(solution)/shard_map/reduce_scatter | solution.py:72
  182.6 25.1 %reduce-scatter.8.cloned.1.call-done = bf16[8,1024]{1,0:T(8,128)(2,1)} async-done(((bf16[32,1024]{1,0:T(8,128)(2,1)}), bf16[8,1024]{1,0:T(8,128)(2,1)}) %reduce-scatter.8.cloned.1.call-update) | async-done | bytes 16400 | tf_op jit(solution)/shard_map/reduce_scatter | solution.py:72
  207.7 0.7 broadcast_in_dim.25
  208.4 6.3 %all_to_all.32 = bf16[2,8,1024]{2,1,0:T(8,128)(2,1)S(1)} all-to-all(bf16[2,8,1024]{2,1,0:T(8,128)(2,1)S(1)} %broadcast_in_dim.25), channel_id=1, replica_groups=mesh['ep_0'=8,'ep_1'=4,'ep_2'=4,'tp'=2] {'tp'}, dimensions={0} | all-to-all | bytes 65536 | tf_op jit(solution)/shard_map/all_to_all | solution.py:33
  214.8 0.6 fusion.39
  (66 shorter events, 0.9 us)
Async XLA Ops:
  7.2 128.6 %copy-start = (bf16[1,256,1024]{2,1,0:T(8,128)(2,1)S(1)}, bf16[1,256,1024]{2,1,0:T(8,128)(2,1)}, u32[]{:S(2)}) copy-start(bf16[1,256,1024]{2,1,0:T(8,128)(2,1)} %param.37) | copy-start | bytes 1572868
  20.1 3.3 %copy-start.10 = (f32[2]{0:T(128)S(1)}, f32[2]{0:T(128)}, u32[]{:S(2)}) copy-start(f32[2]{0:T(128)} %param.29) | copy-start | bytes 28
  20.1 3.5 %copy-start.4 = (bf16[16,1024]{1,0:T(8,128)(2,1)S(1)}, bf16[16,1024]{1,0:T(8,128)(2,1)}, u32[]{:S(2)}) copy-start(bf16[16,1024]{1,0:T(8,128)(2,1)} %param.21) | copy-start | bytes 98308
  20.1 3.5 %copy-start.14 = (bf16[1024,128]{1,0:T(8,128)(2,1)S(1)}, bf16[1024,128]{1,0:T(8,128)(2,1)}, u32[]{:S(2)}) copy-start(bf16[1024,128]{1,0:T(8,128)(2,1)} %param.28) | copy-start | bytes 786436
  24.5 3.1 %copy-start.15 = (bf16[128]{0:T(256)(128)(2,1)S(1)}, bf16[128]{0:T(256)(128)(2,1)}, u32[]{:S(2)}) copy-start(bf16[128]{0:T(256)(128)(2,1)} %param.30) | copy-start | bytes 772
  24.5 3.2 %copy-start.2 = (bf16[256,1024]{1,0:T(8,128)(2,1)S(1)}, bf16[256,1024]{1,0:T(8,128)(2,1)}, u32[]{:S(2)}) copy-start(bf16[256,1024]{1,0:T(8,128)(2,1)} %param.31) | copy-start | bytes 1572868
  24.5 11.7 %copy-start.11 = (bf16[1024]{0:T(1024)(128)(2,1)S(1)}, bf16[1024]{0:T(1024)(128)(2,1)}, u32[]{:S(2)}) copy-start(bf16[1024]{0:T(1024)(128)(2,1)} %param.32) | copy-start | bytes 6148
  24.5 31.0 %copy-start.12 = (bf16[1024]{0:T(1024)(128)(2,1)S(1)}, bf16[1024]{0:T(1024)(128)(2,1)}, u32[]{:S(2)}) copy-start(bf16[1024]{0:T(1024)(128)(2,1)} %param.41) | copy-start | bytes 6148
  24.5 31.0 %copy-start.5 = (bf16[16,1024]{1,0:T(8,128)(2,1)S(1)}, bf16[16,1024]{1,0:T(8,128)(2,1)}, u32[]{:S(2)}) copy-start(bf16[16,1024]{1,0:T(8,128)(2,1)} %param.40) | copy-start | bytes 98308
  24.6 31.0 %copy-start.6 = (bf16[1024,16]{0,1:T(8,128)(2,1)S(1)}, bf16[1024,16]{0,1:T(8,128)(2,1)}, u32[]{:S(2)}) copy-start(bf16[1024,16]{0,1:T(8,128)(2,1)} %param.39) | copy-start | bytes 98308
  24.6 31.0 %copy-start.7 = (bf16[1024,16]{0,1:T(8,128)(2,1)S(1)}, bf16[1024,16]{0,1:T(8,128)(2,1)}, u32[]{:S(2)}) copy-start(bf16[1024,16]{0,1:T(8,128)(2,1)} %param.38) | copy-start | bytes 98308
  28.6 7.6 %all-to-all-start = ((bf16[2,16,1024]{2,1,0:T(8,128)(2,1)}), bf16[2,16,1024]{2,1,0:T(8,128)(2,1)S(1)}, u32[]{:S(2)}, u32[]{:S(2)}) async-start(bf16[2,16,1024]{2,1,0:T(8,128)(2,1)} %broadcast_in_dim.22), calls=%async_computation | async-start | bytes 131072 | tf_op jit(solution)/shard_map/all_to_all | solution.py:33
  35.0 63.5 %all-gather.2.cloned.1.call-start = ((), (), s32[]{:S(2)}) async-start(), calls=%async_computation.9 | async-start | bytes 2359296 | tf_op jit(solution)/shard_map/all_gather | solution.py:65
  55.5 102.9 %reduce-scatter.4.cloned.1.call-start = ((), (), s32[]{:S(2)}) async-start(), calls=%async_computation.10 | async-start | bytes 2359296 | tf_op jit(solution)/shard_map/reduce_scatter | solution.py:72
  98.5 2.4 %copy-start.1 = (bf16[1024,1024]{1,0:T(8,128)(2,1)S(1)}, bf16[1024,1024]{1,0:T(8,128)(2,1)}, u32[]{:S(2)}) copy-start(bf16[1024,1024]{1,0:T(8,128)(2,1)} %all-gather.2.cloned.1.call-done) | copy-start | bytes 6291460
  104.4 0.7 copy-start.8
  105.1 30.3 %copy-start.3 = (bf16[1,1024,256]{2,1,0:T(8,128)(2,1)S(1)}, bf16[1,1024,256]{2,1,0:T(8,128)(2,1)}, u32[]{:S(2)}) copy-start(bf16[1,1024,256]{2,1,0:T(8,128)(2,1)} %param.35) | copy-start | bytes 1572868
  106.1 29.6 %copy-start.13 = (bf16[1,1024,256]{2,1,0:T(8,128)(2,1)S(1)}, bf16[1,1024,256]{2,1,0:T(8,128)(2,1)}, u32[]{:S(2)}) copy-start(bf16[1,1024,256]{2,1,0:T(8,128)(2,1)} %param.36) | copy-start | bytes 1572868
  136.5 21.9 %copy-start.9 = (f32[16,6]{0,1:T(8,128)S(1)}, f32[16,6]{0,1:T(8,128)}, u32[]{:S(2)}) copy-start(f32[16,6]{0,1:T(8,128)} %param.34) | copy-start | bytes 1156
  151.2 20.1 %all-to-all-start.3 = ((bf16[128,2,512]{2,1,0:T(2,128)(2,1)}), bf16[128,2,512]{2,1,0:T(2,128)(2,1)S(1)}, u32[]{:S(2)}, u32[]{:S(2)}) async-start(bf16[128,2,512]{2,1,0:T(2,128)(2,1)} %reshape.285), calls=%async_computation.3 | async-start | bytes 524288 | tf_op jit(solution)/shard_map/all_to_all | solution.py:123
  157.4 25.1 %reduce-scatter.6.cloned.1.call-start = ((), (), s32[]{:S(2)}) async-start(), calls=%async_computation.11 | async-start | bytes 327680 | tf_op jit(solution)/shard_map/reduce_scatter | solution.py:72
  172.3 10.2 %all-to-all-start.4 = ((bf16[2,16,512]{2,1,0:T(8,128)(2,1)}), bf16[2,16,512]{2,1,0:T(8,128)(2,1)S(1)}, u32[]{:S(2)}, u32[]{:S(2)}) async-start(bf16[2,16,512]{2,1,0:T(8,128)(2,1)} %broadcast_in_dim.24), calls=%async_computation.4 | async-start | bytes 65536 | tf_op jit(solution)/shard_map/all_to_all | solution.py:33
  177.7 30.0 %reduce-scatter.8.cloned.1.call-start = ((), (), s32[]{:S(2)}) async-start(), calls=%async_computation.12 | async-start | bytes 81920 | tf_op jit(solution)/shard_map/reduce_scatter | solution.py:72
Sparse Core Ops, SparseCore 0:
  55.6 42.9 all-gather.1
  104.6 48.8 reduce-scatter.3
  160.7 21.7 reduce-scatter.5
  184.9 22.7 reduce-scatter.7
where the time goes:
time: 223 us; the launch traced here: 222 us
  waiting for transfers between devices  79.1 us (35%)
  blocking collectives  75.8 us (34%)
  starting transfers between devices  18.1 us (8%)
  matrix products  17.3 us (8%)
  between operations  14.2 us (6%)
  local copies, waits for them, and re-layouts  12.1 us (5%)
  other arithmetic  5.27 us (2%)
    all_gather x1, waiting for transfers between devices, whole_of(): nearer = lax.all_gather(shard, axes[-1], axis=dim, tiled=True)  35.2 us
    reduce_scatter x3, waiting for transfers between devices, summed_rows(): nearer = lax.psum_scatter(shard, axes[0], scatter_dimension=dim, tiled=True)  29.9 us
    all_to_all x1, blocking collectives, per_device(): lax.all_to_all(outgoing, EP, split_axis=0, concat_axis=0, tiled=True)  28.9 us
    all_gather x2, blocking collectives, whole_of(): nearer = lax.all_gather(shard, axes[-1], axis=dim, tiled=True)  19.1 us
    all_to_all x1, blocking collectives, sum_at_owner(): lax.all_to_all(cut_along(shard, dim, count), axis, 0, 0, tiled=True)  13.8 us
    all_to_all x1, waiting for transfers between devices, serve_slots(): return lax.all_to_all(halved, EP, split_axis=0, concat_axis=0, tiled=True)  12.8 us
    all_to_all x2, starting transfers between devices, sent_to_all(): return lax.all_to_all(copies, axis, split_axis=0, concat_axis=0, tiled=True)  11.9 us
    all_gather x1, blocking collectives, gather_turned(): out, at, done = (lax.all_gather(both, axis, axis=0, tiled=True), 0, [])  7.73 us
  transfers between devices with their start and end apart: 7, of which 5 were waited for; matrix products, arithmetic and copies ran while one was open for 2% of the time, Pallas kernels for 0%

commit v1 on v0

v1 whole, which is shorter than its diff:
```python
import jax
import jax.numpy as jnp
from jax import lax
from jax.experimental import pallas as pl
from jax.experimental.pallas import tpu as pltpu
from jax.sharding import PartitionSpec as P

MESH = pl.DeviceIdType.MESH
BF = jnp.bfloat16
F32 = jnp.float32
EPS = 1e-06
NZ, NY, NX = 8, 4, 4
Z_ORDER = (4, 3, 5, 2, 6, 1, 7, 0)
SEQS, WIDTH, LENGTH = 16, 1024, 1024


def norm(rows, gain):
    scale = lax.rsqrt(jnp.mean(rows * rows, axis=-1, keepdims=True) + EPS)
    return rows * scale * gain


def silu(v):
    return v / (1.0 + jnp.exp(-v))


def body(
    residual, attend_gain, channel_gain, mixer, head_gain, cosine, sine,
    lengths, lambdas, routes, routes_turned, route_weight,
    cache_keys, cache_values, w_query, w_key, w_value, w_out,
    e_gate, e_up, e_down, d_gate, d_up, d_down,
    out, new_keys, new_values,
    kbuf, vbuf, wq, wk, wv, wo, egb, eub, edb, dwb,
    qs, kn, nv, att, pa, pb, nsb, sc, snd, rcv, snd2, rcv2, dtok, dps, dpr, fin_s, fin_r,
    load_sem, k_sem, v_sem, own_sem, zs_sem, zr_sem, ps_sem, pr_sem, es_sem, er_sem,
    xs_sem, xr_sem, ms_sem, mr_sem, ts_sem, tr_sem, bs_sem, br_sem, cs_sem, cr_sem,
    fs_sem, fr_sem,
):
    ep = lax.axis_index("ep")
    c = lax.axis_index("tp")
    z = ep // 16
    y = (ep // 4) % 4
    x = ep % 4
    parity = x % 2
    me = z * 8 + y * 2 + x // 2
    self_in = parity == c
    other = (ep, 1 - c)

    def partner(n):
        return ((n // 8) * 16 + ((n // 2) % 4) * 4 + (n % 2) * 2 + c, parity)

    def is_self(n):
        return jnp.logical_and(self_in, n == me)

    def z_peer(d):
        return (((z + d) % NZ) * 16 + y * 4 + x, c)

    def near(zz, k):
        return zz * 8 + ((y + k // 2) % 4) * 2 + (x // 2 + k % 2) % 2

    barrier = pltpu.get_barrier_semaphore()
    for dz in Z_ORDER:
        zz = (z + dz) % NZ

        @pl.loop(0, 8)
        def _(k):
            n = near(zz, 7 - k)

            @pl.when(jnp.logical_not(is_self(n)))
            def _():
                pl.semaphore_signal(barrier, inc=1, device_id=partner(n), device_id_type=MESH)

    for d in range(1, 8):
        pl.semaphore_signal(barrier, inc=1, device_id=z_peer(d), device_id_type=MESH)
    pl.semaphore_signal(barrier, inc=1, device_id=other, device_id_type=MESH)

    loads = [
        pltpu.make_async_copy(src, dst, load_sem.at[i])
        for i, (src, dst) in enumerate(
            [(w_query, wq), (w_key, wk), (w_value, wv), (w_out, wo),
             (e_gate, egb.at[c]), (e_up, eub.at[c]), (e_down, edb.at[c])]
        )
    ]
    own_parts = [
        pltpu.make_async_copy(src, dwb.at[z, c, i], own_sem.at[i])
        for i, src in enumerate([d_gate, d_up, d_down])
    ]
    kv = [
        (
            pltpu.make_async_copy(cache_keys.at[s], kbuf.at[s], k_sem.at[s]),
            pltpu.make_async_copy(cache_values.at[s], vbuf.at[s], v_sem.at[s]),
        )
        for s in range(SEQS)
    ]
    for i in range(3):
        loads[i].start()
    for cp in own_parts:
        cp.start()
    for s in range(SEQS):
        kv[s][0].start()
        kv[s][1].start()
    for i in range(3, 7):
        loads[i].start()

    row128 = lax.broadcasted_iota(jnp.int32, (128, SEQS), 0)
    expert_t = (row128 // 2) * 2 + c
    hit_t = jnp.zeros((128, SEQS), F32)
    for k in range(6):
        hit_t = hit_t + jnp.where(routes_turned[k : k + 1, :] == expert_t, 1.0, 0.0)
    up_tri = jnp.where(
        lax.broadcasted_iota(jnp.int32, (SEQS, SEQS), 0)
        < lax.broadcasted_iota(jnp.int32, (SEQS, SEQS), 1),
        1.0, 0.0,
    )
    rank_t = jnp.dot(hit_t.astype(BF), up_tri.astype(BF), preferred_element_type=F32)
    pick_t = jnp.where(rank_t == (row128 % 2).astype(F32), hit_t, 0.0).astype(BF)

    lane128 = lax.broadcasted_iota(jnp.int32, (SEQS, 128), 1)
    expert_l = (lane128 // 2) * 2 + c
    hit_l = jnp.zeros((SEQS, 128), F32)
    weight_l = jnp.zeros((SEQS, 128), F32)
    for k in range(6):
        same = routes[:, k : k + 1] == expert_l
        hit_l = hit_l + jnp.where(same, 1.0, 0.0)
        weight_l = weight_l + jnp.where(same, route_weight[:, k : k + 1], 0.0)
    low_tri = jnp.where(
        lax.broadcasted_iota(jnp.int32, (SEQS, SEQS), 1)
        < lax.broadcasted_iota(jnp.int32, (SEQS, SEQS), 0),
        1.0, 0.0,
    )
    rank_l = jnp.dot(low_tri.astype(BF), hit_l.astype(BF), preferred_element_type=F32)
    combine = jnp.where(rank_l == (lane128 % 2).astype(F32), weight_l, 0.0)
    c_hi = combine.astype(BF)
    rest = combine - c_hi.astype(F32)
    c_mid = rest.astype(BF)
    c_lo = (rest - c_mid.astype(F32)).astype(BF)
    combine3 = jnp.concatenate([c_hi, c_mid, c_lo], axis=0)

    res = residual[...].astype(F32)
    normed = norm(res, attend_gain[...].astype(F32)).astype(BF)
    for i in range(3):
        loads[i].wait()
    q = jnp.dot(normed, wq[...], preferred_element_type=F32)
    kk = jnp.dot(normed, wk[...], preferred_element_type=F32)
    vv = jnp.dot(normed, wv[...], preferred_element_type=F32).astype(BF)
    cos_t, sin_t = cosine[...], sine[...]
    first = (lane128 % 64) < 32

    def rotated(u):
        swapped = jnp.where(first, pltpu.roll(u, 96, 1), pltpu.roll(u, 32, 1))
        return (u * cos_t + swapped * sin_t).astype(BF)

    k_rot = rotated(kk)
    new_keys[...] = k_rot
    new_values[...] = vv
    kn[...] = k_rot.astype(F32)
    nv[...] = vv.astype(F32)
    qs[...] = jnp.zeros((SEQS, 8, 128), F32)
    for g in range(2):
        q_rot = rotated(q[:, 128 * g : 128 * g + 128]).astype(F32) * 0.125
        qs[:, g, :] = jnp.where(lane128 < 64, q_rot, 0.0)
        qs[:, 4 + g, :] = jnp.where(lane128 < 64, 0.0, q_rot)

    sub8 = lax.broadcasted_iota(jnp.int32, (8, 1), 0)
    lam = jnp.where(sub8 == 0, lambdas[0], lambdas[1])
    position = lax.broadcasted_iota(jnp.int32, (8, LENGTH), 1)

    def attend(s):
        kv[s][0].wait()
        query = qs[s]
        scores = lax.dot_general(
            query.astype(BF), kbuf[s], (((1,), (1,)), ((), ())), preferred_element_type=F32
        )
        e = jnp.where(position < lengths[s], jnp.exp(scores), 0.0)
        own = jnp.exp(
            jnp.broadcast_to(jnp.sum(query * kn[s : s + 1, :], axis=-1, keepdims=True), (8, 128))
        )
        inverse = 1.0 / (jnp.sum(e, axis=-1, keepdims=True) + own)
        p = e * inverse[:, 0:1]
        po = own * inverse
        w = (p - lam * pltpu.roll(p, 4, 0)).astype(BF)
        w_own = (po - lam * pltpu.roll(po, 4, 0)).astype(BF).astype(F32)
        kv[s][1].wait()
        att[s] = jnp.dot(w, vbuf[s], preferred_element_type=F32) + w_own * nv[s : s + 1, :]

    for s in range(8):
        attend(s)

    pl.semaphore_wait(barrier, 64 + 7 + 1 - self_in.astype(jnp.int32))

    def z_copy(src, d_at_dest, hop, part=None):
        ref = dwb.at[src, c] if part is None else dwb.at[src, c, part]
        return pltpu.make_async_remote_copy(
            src_ref=ref, dst_ref=ref, send_sem=zs_sem.at[d_at_dest if part is None else 8 + part.start // 2],
            recv_sem=zr_sem.at[d_at_dest if part is None else 8 + part.start // 2],
            device_id=z_peer(hop), device_id_type=MESH,
        )

    for cp in own_parts:
        cp.wait()
    step1 = [z_copy(z, (-h) % 8, h) for h in (2, -2, 1, -1)]
    for cp in step1:
        cp.start()
    swaps = [
        pltpu.make_async_remote_copy(
            src_ref=src, dst_ref=dst.at[c], send_sem=es_sem.at[i], recv_sem=er_sem.at[i],
            device_id=other, device_id_type=MESH,
        )
        for i, (src, dst) in enumerate([(e_gate, egb), (e_up, eub), (e_down, edb)])
    ]
    for cp in swaps:
        cp.start()

    for s in range(8, SEQS):
        attend(s)

    gain_h = head_gain[...].astype(F32)
    rows = jnp.concatenate(
        [(norm(att[:, g, :], gain_h) * 0.8).astype(BF) for g in range(2)], axis=1
    )
    loads[3].wait()
    pa[...] = jnp.dot(rows, wo[...], preferred_element_type=F32).astype(BF)
    swap_a = pltpu.make_async_remote_copy(
        src_ref=pa, dst_ref=pb, send_sem=xs_sem, recv_sem=xr_sem,
        device_id=other, device_id_type=MESH,
    )
    swap_a.start()
    swap_a.wait()
    middle = (res + (pa[...].astype(F32) + pb[...].astype(F32))).astype(BF).astype(F32)
    ns = norm(middle, channel_gain[...].astype(F32)).astype(BF)
    nsb[...] = ns
    switch = jax.nn.sigmoid(
        jnp.sum(ns.astype(F32) * mixer[...].astype(F32), axis=-1, keepdims=True)
    )

    def spread(values):
        for j in range(8):
            sc[pl.ds(j, 128, stride=8), :] = values[:, 128 * j : 128 * j + 128]

    def send_blocks(src, dst, send_sem, recv_sem):
        for dz in Z_ORDER:
            zz = (z + dz) % NZ

            @pl.loop(0, 8)
            def _(k):
                n = near(zz, 7 - k)

                @pl.when(is_self(n))
                def _():
                    pltpu.make_async_copy(src.at[n], dst.at[me], recv_sem.at[z]).start()

                @pl.when(jnp.logical_not(is_self(n)))
                def _():
                    pltpu.make_async_remote_copy(
                        src_ref=src.at[n], dst_ref=dst.at[me], send_sem=send_sem,
                        recv_sem=recv_sem.at[z], device_id=partner(n), device_id_type=MESH,
                    ).start()

    def sent_all(buf, send_sem, count):
        @pl.when(self_in)
        def _():
            part = buf.at[pl.ds(0, count - 1)]
            pltpu.make_async_copy(part, part, send_sem).wait()

        @pl.when(jnp.logical_not(self_in))
        def _():
            pltpu.make_async_copy(buf, buf, send_sem).wait()

    def send_plane(pick_src, dst, send_sem, recv_sem):
        @pl.loop(0, 8)
        def _(k):
            n = near(z, 7 - k)
            src = pick_src(n % 8)

            @pl.when(is_self(n))
            def _():
                pltpu.make_async_copy(src, dst.at[me % 8], recv_sem).start()

            @pl.when(jnp.logical_not(is_self(n)))
            def _():
                pltpu.make_async_remote_copy(
                    src_ref=src, dst_ref=dst.at[me % 8], send_sem=send_sem,
                    recv_sem=recv_sem, device_id=partner(n), device_id_type=MESH,
                ).start()

    spread(jnp.dot(pick_t, ns, preferred_element_type=F32))
    snd[...] = sc[...].reshape(64, 16, 128).astype(BF)
    send_blocks(snd, rcv, ms_sem, mr_sem)
    send_plane(lambda n: nsb, dtok, ts_sem, tr_sem)

    for d in (7, 6, 1, 2):
        src = (z + d) % NZ
        pltpu.make_async_copy(dwb.at[src, c], dwb.at[src, c], zr_sem.at[d]).wait()
    step2 = [
        z_copy((z + 2) % 8, 4, -2, pl.ds(0, 2)),
        z_copy((z - 2) % 8, 4, 2, pl.ds(2, 1)),
        z_copy((z + 2) % 8, 3, -1),
        z_copy((z - 2) % 8, 5, 1),
    ]
    for cp in step2:
        cp.start()

    def forward(d):
        ref = dwb.at[(z + d) % NZ, c]
        return pltpu.make_async_remote_copy(
            src_ref=ref, dst_ref=ref, send_sem=ps_sem.at[d], recv_sem=pr_sem.at[d],
            device_id=other, device_id_type=MESH,
        )

    for d in (0, 1, 7, 2, 6):
        forward(d).start()

    for i in range(4, 7):
        loads[i].wait()
    for cp in swaps:
        cp.wait()
    for zz in range(8):
        part = rcv.at[pl.ds(zz * 8, 8)]
        pltpu.make_async_copy(part, part, mr_sem.at[zz]).wait()
    sc[...] = rcv[...].reshape(1024, 128).astype(F32)

    def gathered():
        return jnp.concatenate(
            [sc[pl.ds(j, 128, stride=8), :].astype(BF) for j in range(8)], axis=1
        )

    xr = gathered()
    total = jnp.zeros((128, WIDTH), F32)
    for h in range(2):
        gate = jnp.dot(xr, egb[h], preferred_element_type=F32)
        upper = jnp.dot(xr, eub[h], preferred_element_type=F32)
        hidden = (silu(gate) * upper).astype(BF)
        total = total + jnp.dot(hidden, edb[h], preferred_element_type=F32).astype(BF).astype(F32)
    spread(total)
    snd2[...] = sc[...].reshape(64, 16, 128).astype(BF)
    send_blocks(snd2, rcv2, bs_sem, br_sem)

    for d in (3, 5):
        src = (z + d) % NZ
        pltpu.make_async_copy(dwb.at[src, c], dwb.at[src, c], zr_sem.at[d]).wait()
    far = dwb.at[(z + 4) % NZ, c]
    for i, part in enumerate((far.at[pl.ds(0, 2)], far.at[pl.ds(2, 1)])):
        pltpu.make_async_copy(part, part, zr_sem.at[8 + i]).wait()
    for d in (3, 5, 4):
        forward(d).start()
    pltpu.make_async_copy(dtok, dtok, tr_sem).wait()
    for d in range(8):
        mirror = dwb.at[(z + d) % NZ, 1 - c]
        pltpu.make_async_copy(mirror, mirror, pr_sem.at[d]).wait()
    xd = dtok[...].reshape(128, WIDTH)
    turned = (((1,), (1,)), ((), ()))
    gate_w = dwb[:, :, 0].reshape(256, WIDTH)
    up_w = dwb[:, :, 1].reshape(256, WIDTH)
    down_w = dwb[:, :, 2].reshape(256, WIDTH)
    gate = lax.dot_general(xd, gate_w, turned, preferred_element_type=F32)
    upper = lax.dot_general(xd, up_w, turned, preferred_element_type=F32)
    hidden = (silu(gate) * upper).astype(BF)
    dps[...] = jnp.dot(hidden, down_w, preferred_element_type=F32).astype(BF).reshape(8, 16, WIDTH)
    send_plane(lambda n: dps.at[n], dpr, cs_sem, cr_sem)

    for zz in range(8):
        part = rcv2.at[pl.ds(zz * 8, 8)]
        pltpu.make_async_copy(part, part, br_sem.at[zz]).wait()
    sc[...] = rcv2[...].reshape(1024, 128).astype(F32)
    three = jnp.dot(combine3, gathered(), preferred_element_type=F32)
    routed = three[0:16] + (three[16:32] + three[32:48])
    pltpu.make_async_copy(dpr, dpr, cr_sem).wait()
    dense = dpr[0].astype(F32)
    for i in range(1, 8):
        dense = dense + dpr[i].astype(F32)
    fin_s[...] = routed + switch * dense
    swap_f = pltpu.make_async_remote_copy(
        src_ref=fin_s, dst_ref=fin_r, send_sem=fs_sem, recv_sem=fr_sem,
        device_id=other, device_id_type=MESH,
    )
    swap_f.start()
    sent_all(snd, ms_sem, 64)
    sent_all(snd2, bs_sem, 64)
    sent_all(dtok, ts_sem, 8)
    sent_all(dps, cs_sem, 8)
    for cp in step1 + step2:
        cp.wait_send()
    for d in range(8):
        forward(d).wait_send()
    swap_f.wait()
    out[...] = (middle + (fin_s[...] + fin_r[...])).astype(BF)


def per_device(
    residual_in, lengths, cache_keys, cache_values, attend_gain, query_proj, key_proj,
    value_proj, lambdas, head_gain, out_proj, channel_gain, routes, route_weight,
    expert_gate, expert_up, expert_down, dense_gate, dense_up, dense_down, dense_mixer,
):
    inverse = 10000.0 ** (-jnp.arange(32, dtype=F32) / 32)
    angles = lengths.astype(F32)[:, None] * inverse
    cos, sin = jnp.cos(angles), jnp.sin(angles)
    cosine = jnp.concatenate([cos, cos, cos, cos], axis=1)
    sine = jnp.concatenate([-sin, sin, -sin, sin], axis=1)
    vm = pl.BlockSpec(memory_space=pltpu.VMEM)
    sm = pl.BlockSpec(memory_space=pltpu.SMEM)
    hb = pl.BlockSpec(memory_space=pl.ANY)
    DMA = pltpu.SemaphoreType.DMA
    V = pltpu.VMEM
    out, keys, values = pl.pallas_call(
        body,
        name="layer",
        out_shape=(
            jax.ShapeDtypeStruct((SEQS, WIDTH), BF),
            jax.ShapeDtypeStruct((SEQS, 128), BF),
            jax.ShapeDtypeStruct((SEQS, 128), BF),
        ),
        in_specs=[vm] * 7 + [sm] * 2 + [vm] * 3 + [hb] * 12,
        out_specs=(vm, vm, vm),
        scratch_shapes=[
            V((SEQS, LENGTH, 128), BF), V((SEQS, LENGTH, 128), BF),
            V((1024, 256), BF), V((1024, 128), BF), V((1024, 128), BF), V((256, 1024), BF),
            V((2, 1024, 256), BF), V((2, 1024, 256), BF), V((2, 256, 1024), BF),
            V((8, 2, 3, 16, 1024), BF),
            V((SEQS, 8, 128), F32), V((SEQS, 128), F32), V((SEQS, 128), F32),
            V((SEQS, 8, 128), F32),
            V((SEQS, WIDTH), BF), V((SEQS, WIDTH), BF), V((SEQS, WIDTH), BF),
            V((1024, 128), F32),
            V((64, 16, 128), BF), V((64, 16, 128), BF), V((64, 16, 128), BF), V((64, 16, 128), BF),
            V((8, 16, WIDTH), BF), V((8, 16, WIDTH), BF), V((8, 16, WIDTH), BF),
            V((SEQS, WIDTH), F32), V((SEQS, WIDTH), F32),
            DMA((7,)), DMA((16,)), DMA((16,)), DMA((3,)),
            DMA((10,)), DMA((10,)), DMA((8,)), DMA((8,)), DMA((3,)), DMA((3,)),
            DMA, DMA, DMA, DMA((8,)), DMA, DMA, DMA, DMA((8,)), DMA, DMA,
            DMA, DMA,
        ],
        compiler_params=pltpu.CompilerParams(
            collective_id=0, has_side_effects=True, vmem_limit_bytes=60 * 1024 * 1024
        ),
    )(
        residual_in, attend_gain.reshape(1, -1), channel_gain.reshape(1, -1),
        dense_mixer.reshape(1, -1), head_gain.reshape(1, -1), cosine, sine,
        lengths, lambdas, routes, routes.T, route_weight,
        cache_keys.reshape(SEQS, LENGTH, 128), cache_values.reshape(SEQS, LENGTH, 128),
        query_proj, key_proj, value_proj, out_proj,
        expert_gate[0], expert_up[0], expert_down[0], dense_gate.T, dense_up.T, dense_down,
    )
    return out, keys.reshape(SEQS, 1, 128), values.reshape(SEQS, 1, 128)


def solution(mesh):
    placed = (
        P("ep", None), P("ep"), P("ep", "tp", None, None), P("ep", "tp", None, None), P(),
        P(None, "tp"), P(None, "tp"), P(None, "tp"), P("tp"), P(), P("tp", None), P(),
        P("ep", None), P("ep", None), P("ep", None, "tp"), P("ep", None, "tp"),
        P("ep", "tp", None), P(None, ("ep", "tp")), P(None, ("ep", "tp")),
        P(("ep", "tp"), None), P(),
    )
    return jax.shard_map(
        per_device, mesh=mesh, in_specs=placed,
        out_specs=(P("ep", None), P("ep", "tp", None), P("ep", "tp", None)),
        check_vma=False,
    )
```

time: 223 us -> 62.2 us (0.28)
  waiting for transfers between devices: 79.1 us -> 0 us
  blocking collectives: 75.8 us -> 0 us
  Pallas kernels: 0 us -> 49.2 us
  starting transfers between devices: 18.1 us -> 0 us
  matrix products: 17.3 us -> 0 us
  between operations: 14.2 us -> 0.65 us
  other arithmetic: 5.27 us -> 1.47 us
    pallas_call x0 -> x1, Pallas kernels: none -> 49.2 us  [per_device(): pl.pallas_call(body, name='layer', out_shape=(jax.ShapeDtypeStruct((SEQS,...]
    all_to_all x3 -> x0, blocking collectives: 49 us -> none  [the longest x1 28.9 us: per_device(): lax.all_to_all(outgoing, EP, split_axis=0, concat_axis=0, tiled=True)]
    all_gather x1 -> x0, waiting for transfers between devices: 35.2 us -> none  [whole_of(): nearer = lax.all_gather(shard, axes[-1], axis=dim, tiled=True)]
    reduce_scatter x3 -> x0, waiting for transfers between devices: 29.9 us -> none  [summed_rows(): nearer = lax.psum_scatter(shard, axes[0], scatter_dimension=dim, tiled=True)]
    all_gather x3 -> x0, blocking collectives: 26.8 us -> none  [the longest x2 19.1 us: whole_of(): nearer = lax.all_gather(shard, axes[-1], axis=dim, tiled=True)]
    all_to_all x3 -> x0, starting transfers between devices: 18 us -> none  [the longest x2 11.9 us: sent_to_all(): return lax.all_to_all(copies, axis, split_axis=0, concat_axis=0, tiled=True)]
    dot_general x14 -> x0, matrix products: 17.3 us -> none  [the longest x1 3.08 us: per_device(): jnp.einsum('sagmd,salmd->sagml', queries, cached, preferred_element_type=...]
    all_to_all x3 -> x0, waiting for transfers between devices: 13.9 us -> none  [the longest x1 12.8 us: serve_slots(): return lax.all_to_all(halved, EP, split_axis=0, concat_axis=0, tiled=True)]
  transfers between devices with their start and end apart: 7 -> 0, of which waited for: 5 -> 0; matrix products, arithmetic and copies ran while one was open for 2% -> 0% of each run, Pallas kernels for 0% -> 0%
where the time goes in v1:
time: 62.2 us; the launch traced here: 61.8 us
  Pallas kernels  49.2 us (79%)
  local copies, waits for them, and re-layouts  10.5 us (17%)
  other arithmetic  1.47 us (2%)
  between operations  0.65 us (1%)
    pallas_call x1, Pallas kernels, per_device(): pl.pallas_call(body, name='layer', out_shape=(jax.ShapeDtypeStruct((SEQS,...  49.2 us
    unnamed x5, local copies, waits for them, and re-layouts  6.64 us
    reshape x1, local copies, waits for them, and re-layouts, per_device(): attend_gain.reshape(1, -1)  1.28 us
    reshape x1, local copies, waits for them, and re-layouts, per_device(): channel_gain.reshape(1, -1)  1.28 us
    reshape x1, local copies, waits for them, and re-layouts, per_device(): dense_mixer.reshape(1, -1)  1.27 us

profile of v1, /device:TPU:1, one launch (start us, length us, event | category | flops | bytes accessed | tf_op | source)
XLA Modules:
  0.0 61.8 jit_solution(13959568893895595582)
XLA Ops:
  0.6 0.7 %convert_element_type.3 = f32[16]{0:T(128)S(1)} convert(s32[16]{0:T(128)} %lengths.1) | non-fusion elementwise | flops 16 | bytes 128 | tf_op jit(solution)/shard_map/convert_element_type | solution.py:394
  1.3 1.3 %reshape.37.attend_gain = bf16[1,1024]{1,0:T(2,128)(2,1)} reshape(bf16[1024]{0:T(1024)(128)(2,1)} %param.25) | data formatting | bytes 4096 | tf_op jit(solution)/shard_map/reshape | solution.py:434
  2.6 1.3 %reshape.38.channel_gain = bf16[1,1024]{1,0:T(2,128)(2,1)} reshape(bf16[1024]{0:T(1024)(128)(2,1)} %param.32) | data formatting | bytes 4096 | tf_op jit(solution)/shard_map/reshape | solution.py:434
  3.9 1.3 %reshape.39.mixer = bf16[1,1024]{1,0:T(2,128)(2,1)} reshape(bf16[1024]{0:T(1024)(128)(2,1)} %param.41) | data formatting | bytes 4096 | tf_op jit(solution)/shard_map/reshape | solution.py:435
  5.1 1.4 %copy.25.route_weight = f32[16,6]{1,0:T(8,128)} copy(f32[16,6]{0,1:T(8,128)} %param.34) | data formatting | bytes 768 | tf_op args[13]
  6.5 1.4 %copy.24.routes = s32[16,6]{1,0:T(8,128)} copy(s32[16,6]{0,1:T(8,128)} %param.33) | data formatting | bytes 768 | tf_op args[12]
  7.9 0.1 fusion
  8.0 0.7 %pad_maximum_fusion = (f32[16,128]{1,0:T(8,128)}, f32[16,128]{1,0:T(8,128)}) fusion(f32[16,32]{1,0:T(8,128)S(1)} %get-tuple-element.11, f32[16,32]{1,0:T(8,128)S(1)} %get-tuple-element.10, f32[16,32]{1,0:T(8,128)S(1)} %get-tuple-element.9), kind=kLoop, calls=%fused_computation.2 | loop fusion | flops 12288 | bytes 22528 | tf_op jit(solution)/shard_map/concatenate | solution.py:396
  8.7 49.2 %layer.1 = (bf16[16,1024]{1,0:T(8,128)(2,1)}, bf16[16,128]{1,0:T(8,128)(2,1)}, bf16[16,128]{1,0:T(8,128)(2,1)}) custom-call(bf16[16,1024]{1,0:T(8,128)(2,1)} %residual.1, bf16[1,1024]{1,0:T(2,128)(2,1)} %reshape.37.attend_gain, bf16[1,1024]{1,0:T(2,128)(2,1)} %reshape.38.channel_gain, bf16[1,1024]{1,0:T(2,128)(2,1)} %reshape.39.mixer, ...), custom_call_target="tpu_custom_call" | custom-call | tf_op jit(solution)/shard_map/layer/pallas_call | solution.py:403
  57.8 1.4 %copy.29 = bf16[16,1024]{1,0:T(8,128)(2,1)} copy(bf16[16,1024]{1,0:T(8,128)(2,1)} %get-tuple-element.17) | data formatting | bytes 65536
  59.2 1.3 %copy.30 = bf16[16,1,128]{2,0,1:T(8,128)(2,1)} copy(bf16[16,1,128]{2,0,1:T(8,128)(2,1)} %bitcast.20) | data formatting | bytes 8192
  60.5 1.3 %copy.31 = bf16[16,1,128]{2,0,1:T(8,128)(2,1)} copy(bf16[16,1,128]{2,0,1:T(8,128)(2,1)} %bitcast.19) | data formatting | bytes 8192
  (1 shorter events, 0.0 us)

commit v2 on v1

v2 whole, which is shorter than its diff:
```python
import jax
import jax.numpy as jnp
import numpy as np
from jax import lax
from jax.experimental import pallas as pl
from jax.experimental.pallas import tpu as pltpu
from jax.sharding import PartitionSpec as P

MESH = pl.DeviceIdType.MESH
BF = jnp.bfloat16
F32 = jnp.float32
EPS = 1e-06
NZ, NY, NX = 8, 4, 4
SEQS, WIDTH, LENGTH = 16, 1024, 1024


def norm(rows, gain):
    scale = lax.rsqrt(jnp.mean(rows * rows, axis=-1, keepdims=True) + EPS)
    return rows * scale * gain


def silu(v):
    return v / (1.0 + jnp.exp(-v))


def body(
    residual, attend_gain, channel_gain, mixer, head_gain, frequency,
    lengths, lambdas, routes_turned, weight_turned,
    cache_keys, cache_values, w_query, w_key, w_value, w_out,
    e_gate, e_up, e_down, d_gate, d_up, d_down,
    out, new_keys, new_values,
    kbuf, vbuf, wq, wk, wv, wo, egb, eub, edb, dwb,
    qs, kn, nv, att, pa, pb, nsb, sc, snd, rcv, snd2, rcv2, dtok, dps, dpr, fin_s, fin_r,
    load_sem, k_sem, v_sem, own_sem, zs_sem, zr_sem, ps_sem, pr_sem, es_sem, er_sem,
    xs_sem, xr_sem, ms_sem, mr_sem, ts_sem, tr_sem, bs_sem, br_sem, cs_sem, cr_sem,
    fs_sem, fr_sem, line_sem,
):
    ep = lax.axis_index("ep")
    c = lax.axis_index("tp")
    z = ep // 16
    y = (ep // 4) % 4
    x = ep % 4
    parity = x % 2
    me = z * 8 + y * 2 + x // 2
    self_in = parity == c
    other = (ep, 1 - c)

    plane = []
    for k in range(8):
        yy = (y + 3 - k // 2) % 4
        xh = (x // 2 + 1 - k % 2) % 2
        plane.append((yy * 4 + xh * 2 + c, yy * 2 + xh))
    mine = me % 8

    def z_peer(d):
        return (((z + d) % NZ) * 16 + y * 4 + x, c)

    loads = [
        pltpu.make_async_copy(src, dst, load_sem.at[i])
        for i, (src, dst) in enumerate(
            [(w_query, wq), (w_key, wk), (w_value, wv), (w_out, wo),
             (e_gate, egb.at[c]), (e_up, eub.at[c]), (e_down, edb.at[c])]
        )
    ]
    own_parts = [
        pltpu.make_async_copy(src, dwb.at[z, c, i], own_sem.at[i])
        for i, src in enumerate([d_gate, d_up, d_down])
    ]
    kv = [
        (
            pltpu.make_async_copy(cache_keys.at[s], kbuf.at[s], k_sem.at[s]),
            pltpu.make_async_copy(cache_values.at[s], vbuf.at[s], v_sem.at[s]),
        )
        for s in range(SEQS)
    ]
    for cp in own_parts:
        cp.start()
    for i in range(3):
        loads[i].start()

    def stream(sequences):
        for kind in range(2):
            for s in sequences:
                kv[s][kind].start()

    stream(range(8))

    barrier = pltpu.get_barrier_semaphore()
    for d in (4, 3, 5, 2, 6, 1, 7):
        pl.semaphore_signal(barrier, inc=1, device_id=z_peer(d), device_id_type=MESH)
    for chip, slot in plane:

        @pl.when(jnp.logical_not(jnp.logical_and(self_in, slot == mine)))
        def _(chip=chip):
            pl.semaphore_signal(barrier, inc=1, device_id=(z * 16 + chip, parity), device_id_type=MESH)

    pl.semaphore_signal(barrier, inc=1, device_id=other, device_id_type=MESH)

    row128 = lax.broadcasted_iota(jnp.int32, (128, SEQS), 0)
    expert_t = (row128 // 2) * 2 + c
    hit_t = jnp.zeros((128, SEQS), F32)
    weight_t = jnp.zeros((128, SEQS), F32)
    for k in range(6):
        same = routes_turned[k : k + 1, :] == expert_t
        hit_t = hit_t + jnp.where(same, 1.0, 0.0)
        weight_t = weight_t + jnp.where(same, weight_turned[k : k + 1, :], 0.0)
    up_tri = jnp.where(
        lax.broadcasted_iota(jnp.int32, (SEQS, SEQS), 0)
        < lax.broadcasted_iota(jnp.int32, (SEQS, SEQS), 1),
        1.0, 0.0,
    )
    rank_t = jnp.dot(hit_t.astype(BF), up_tri.astype(BF), preferred_element_type=F32)
    pick_t = jnp.where(rank_t == (row128 % 2).astype(F32), hit_t, 0.0).astype(BF)

    combine_t = jnp.where(rank_t == (row128 % 2).astype(F32), weight_t, 0.0)
    c_hi = combine_t.astype(BF)
    rest = combine_t - c_hi.astype(F32)
    c_mid = rest.astype(BF)
    c_lo = (rest - c_mid.astype(F32)).astype(BF)
    eye = jnp.where(
        lax.broadcasted_iota(jnp.int32, (SEQS, SEQS), 0)
        == lax.broadcasted_iota(jnp.int32, (SEQS, SEQS), 1),
        1.0, 0.0,
    ).astype(BF)
    combine3 = jnp.concatenate(
        [
            lax.dot_general(eye, part, (((1,), (1,)), ((), ())), preferred_element_type=F32)
            for part in (c_hi, c_mid, c_lo)
        ],
        axis=0,
    ).astype(BF)

    stream(range(8, SEQS))
    loads[3].start()

    res = residual[...].astype(F32)
    normed = norm(res, attend_gain[...].astype(F32).reshape(1, WIDTH)).astype(BF)
    for i in range(3):
        loads[i].wait()
    q = jnp.dot(normed, wq[...], preferred_element_type=F32)
    kk = jnp.dot(normed, wk[...], preferred_element_type=F32)
    vv = jnp.dot(normed, wv[...], preferred_element_type=F32).astype(BF)
    lane128 = lax.broadcasted_iota(jnp.int32, (SEQS, 128), 1)
    row16 = lax.broadcasted_iota(jnp.int32, (SEQS, 128), 0)
    first = (lane128 % 64) < 32
    place = jnp.zeros((SEQS, 128), jnp.int32)
    for s in range(SEQS):
        place = jnp.where(row16 == s, lengths[s], place)
    angles = place.astype(F32) * frequency[...]
    cos_t, sin_t = jnp.cos(angles), jnp.sin(angles)
    sin_t = jnp.where(first, -sin_t, sin_t)

    def rotated(u):
        swapped = jnp.where(first, pltpu.roll(u, 96, 1), pltpu.roll(u, 32, 1))
        return (u * cos_t + swapped * sin_t).astype(BF)

    k_rot = rotated(kk)
    new_keys[...] = k_rot
    new_values[...] = vv
    kn[...] = k_rot.astype(F32)
    nv[...] = vv.astype(F32)
    for g in range(2):
        q_rot = rotated(q[:, 128 * g : 128 * g + 128]).astype(F32) * 0.125
        qs[pl.ds(g, SEQS, stride=4), :] = jnp.where(lane128 < 64, q_rot, 0.0)
        qs[pl.ds(2 + g, SEQS, stride=4), :] = jnp.where(lane128 < 64, 0.0, q_rot)

    pl.semaphore_wait(barrier, 7 + 8 + 1 - self_in.astype(jnp.int32))
    for d in (4, 3, 5, 2, 6, 1, 7):
        pl.semaphore_signal(line_sem, inc=1, device_id=z_peer(d), device_id_type=MESH)

    def z_copy(d, hop):
        ref = dwb.at[(z + hop + d) % NZ, c]
        return pltpu.make_async_remote_copy(
            src_ref=ref, dst_ref=ref, send_sem=zs_sem.at[d], recv_sem=zr_sem.at[d],
            device_id=z_peer(hop), device_id_type=MESH,
        )

    def z_wait(d):
        ref = dwb.at[(z + d) % NZ, c]
        pltpu.make_async_copy(ref, ref, zr_sem.at[d % NZ]).wait()

    def forward(d):
        ref = dwb.at[(z + d) % NZ, c]
        return pltpu.make_async_remote_copy(
            src_ref=ref, dst_ref=ref, send_sem=ps_sem.at[d], recv_sem=pr_sem.at[d],
            device_id=other, device_id_type=MESH,
        )

    for cp in own_parts:
        cp.wait()
    step1 = [z_copy(4, 4), z_copy(7, 1), z_copy(1, -1)]
    for cp in step1:
        cp.start()
    swaps = [
        pltpu.make_async_remote_copy(
            src_ref=src, dst_ref=dst.at[c], send_sem=es_sem.at[i], recv_sem=er_sem.at[i],
            device_id=other, device_id_type=MESH,
        )
        for i, (src, dst) in enumerate([(e_gate, egb), (e_up, eub), (e_down, edb)])
    ]
    forward(0).start()

    sub8 = lax.broadcasted_iota(jnp.int32, (8, 1), 0)
    low8 = sub8 < 4
    lam = jnp.where(sub8 % 2 == 0, lambdas[0], lambdas[1])
    position = lax.broadcasted_iota(jnp.int32, (8, LENGTH), 1)
    turned = (((1,), (1,)), ((), ()))

    def attend(pairs):
        for p in pairs:
            kv[2 * p][0].wait()
            kv[2 * p + 1][0].wait()
        scores, own = [], []
        for p in pairs:
            query = qs[8 * p : 8 * p + 8, :]
            first_q = jnp.where(low8, query, 0.0).astype(BF)
            second_q = jnp.where(low8, 0.0, query).astype(BF)
            scores.append(
                lax.dot_general(first_q, kbuf[2 * p], turned, preferred_element_type=F32)
                + lax.dot_general(second_q, kbuf[2 * p + 1], turned, preferred_element_type=F32)
            )
            key = jnp.where(low8, kn[2 * p : 2 * p + 1, :], kn[2 * p + 1 : 2 * p + 2, :])
            own.append(
                jnp.exp(jnp.broadcast_to(jnp.sum(query * key, axis=-1, keepdims=True), (8, 128)))
            )
        weights, own_weights = [], []
        for i, p in enumerate(pairs):
            limit = jnp.where(low8, lengths[2 * p], lengths[2 * p + 1])
            e = jnp.where(position < limit, jnp.exp(scores[i]), 0.0)
            inverse = 1.0 / (jnp.sum(e, axis=-1, keepdims=True) + own[i])
            share = e * inverse[:, 0:1]
            share_own = own[i] * inverse
            weights.append((share - lam * pltpu.roll(share, 6, 0)).astype(BF))
            own_weights.append(
                (share_own - lam * pltpu.roll(share_own, 6, 0)).astype(BF).astype(F32)
            )
        for p in pairs:
            kv[2 * p][1].wait()
            kv[2 * p + 1][1].wait()
        for i, p in enumerate(pairs):
            first_a = jnp.dot(weights[i], vbuf[2 * p], preferred_element_type=F32)
            second_a = jnp.dot(weights[i], vbuf[2 * p + 1], preferred_element_type=F32)
            value = jnp.where(low8, nv[2 * p : 2 * p + 1, :], nv[2 * p + 1 : 2 * p + 2, :])
            att[8 * p : 8 * p + 8, :] = (
                jnp.where(low8, first_a, second_a) + own_weights[i] * value
            )

    attend((0, 1, 2, 3))
    for i in range(4, 7):
        loads[i].start()

    attend((4, 5, 6, 7))

    gain_h = head_gain[...].astype(F32).reshape(1, 128)
    rows = jnp.concatenate(
        [(norm(att[pl.ds(g, SEQS, stride=4), :], gain_h) * 0.8).astype(BF) for g in range(2)], axis=1
    )
    loads[3].wait()
    pa[...] = jnp.dot(rows, wo[...], preferred_element_type=F32).astype(BF)
    swap_a = pltpu.make_async_remote_copy(
        src_ref=pa, dst_ref=pb, send_sem=xs_sem, recv_sem=xr_sem,
        device_id=other, device_id_type=MESH,
    )
    swap_a.start()
    for cp in swaps:
        cp.start()
    swap_a.wait()
    middle = (res + (pa[...].astype(F32) + pb[...].astype(F32))).astype(BF).astype(F32)
    ns = norm(middle, channel_gain[...].astype(F32).reshape(1, WIDTH)).astype(BF)
    nsb[...] = ns
    switch = jax.nn.sigmoid(
        jnp.sum(ns.astype(F32) * mixer[...].astype(F32).reshape(1, WIDTH), axis=-1, keepdims=True)
    )

    def spread(values):
        for j in range(8):
            sc[pl.ds(j, 128, stride=8), :] = values[:, 128 * j : 128 * j + 128]

    def send_blocks(src, dst, send_sem, recv_sem, distances):
        for dz in distances:
            zz = (z + dz) % NZ
            for chip, slot in plane:
                n = zz * 8 + slot
                remote = pltpu.make_async_remote_copy(
                    src_ref=src.at[n], dst_ref=dst.at[me], send_sem=send_sem,
                    recv_sem=recv_sem.at[z], device_id=(zz * 16 + chip, parity),
                    device_id_type=MESH,
                )
                if dz:
                    remote.start()
                    continue
                self_block = jnp.logical_and(self_in, slot == mine)

                @pl.when(self_block)
                def _(n=n):
                    pltpu.make_async_copy(src.at[n], dst.at[me], recv_sem.at[z]).start()

                @pl.when(jnp.logical_not(self_block))
                def _(remote=remote):
                    remote.start()

    def sent_all(buf, send_sem, count):
        @pl.when(self_in)
        def _():
            part = buf.at[pl.ds(0, count - 1)]
            pltpu.make_async_copy(part, part, send_sem).wait()

        @pl.when(jnp.logical_not(self_in))
        def _():
            pltpu.make_async_copy(buf, buf, send_sem).wait()

    def send_plane(pick_src, dst, send_sem, recv_sem):
        for chip, slot in plane:
            src = pick_src(slot)
            self_block = jnp.logical_and(self_in, slot == mine)

            @pl.when(self_block)
            def _(src=src):
                pltpu.make_async_copy(src, dst.at[mine], recv_sem).start()

            @pl.when(jnp.logical_not(self_block))
            def _(src=src, chip=chip):
                pltpu.make_async_remote_copy(
                    src_ref=src, dst_ref=dst.at[mine], send_sem=send_sem,
                    recv_sem=recv_sem, device_id=(z * 16 + chip, parity), device_id_type=MESH,
                ).start()

    picked = jnp.dot(pick_t, ns, preferred_element_type=F32)
    for j in range(8):
        sc[pl.ds(j, 128, stride=8), :] = picked[:, 128 * j : 128 * j + 128]
    snd[...] = sc[...].reshape(64, 16, 128).astype(BF)
    pl.semaphore_wait(line_sem, 7)
    send_blocks(snd, rcv, ms_sem, mr_sem, (4, 3, 5, 2, 6, 1, 7, 0))
    send_plane(lambda n: nsb, dtok, ts_sem, tr_sem)

    for d in (7, 1, 4):
        z_wait(d)
    step2 = [z_copy(6, 1), z_copy(2, -1), z_copy(3, 1), z_copy(5, -1)]
    for cp in step2:
        cp.start()
    for d in (1, 7, 4):
        forward(d).start()

    for i in range(4, 7):
        loads[i].wait()
    for cp in swaps:
        cp.wait()

    def serve(distances):
        count = len(distances)
        slots = [pl.ds(((z + d) % NZ) * 8, 8) for d in distances]
        for d, part in zip(distances, slots):
            ref = rcv.at[part]
            pltpu.make_async_copy(ref, ref, mr_sem.at[(z + d) % NZ]).wait()
        for i, part in enumerate(slots):
            sc[128 * i : 128 * i + 128, :] = rcv[part].reshape(128, 128).astype(F32)
        rows = jnp.concatenate(
            [sc[pl.ds(j, 16 * count, stride=8), :].astype(BF) for j in range(8)], axis=1
        )
        total = None
        for h in range(2):
            gate = jnp.dot(rows, egb[h], preferred_element_type=F32)
            upper = jnp.dot(rows, eub[h], preferred_element_type=F32)
            hidden = (silu(gate) * upper).astype(BF)
            half = jnp.dot(hidden, edb[h], preferred_element_type=F32).astype(BF).astype(F32)
            total = half if total is None else total + half
        for j in range(8):
            sc[pl.ds(j, 16 * count, stride=8), :] = total[:, 128 * j : 128 * j + 128]
        for i, part in enumerate(slots):
            snd2[part] = sc[128 * i : 128 * i + 128, :].reshape(8, 16, 128).astype(BF)
        send_blocks(snd2, rcv2, bs_sem, br_sem, distances)

    serve((4, 3, 5, 2, 6, 1, 7, 0))

    for d in (2, 6, 3, 5):
        z_wait(d)
        forward(d).start()
    pltpu.make_async_copy(dtok, dtok, tr_sem).wait()
    for d in range(8):
        mirror = dwb.at[(z + d) % NZ, 1 - c]
        pltpu.make_async_copy(mirror, mirror, pr_sem.at[d]).wait()
    xd = dtok[...].reshape(128, WIDTH)
    gate_w = dwb[:, :, 0].reshape(256, WIDTH)
    up_w = dwb[:, :, 1].reshape(256, WIDTH)
    down_w = dwb[:, :, 2].reshape(256, WIDTH)
    gate = lax.dot_general(xd, gate_w, turned, preferred_element_type=F32)
    upper = lax.dot_general(xd, up_w, turned, preferred_element_type=F32)
    hidden = (silu(gate) * upper).astype(BF)
    dps[...] = jnp.dot(hidden, down_w, preferred_element_type=F32).astype(BF).reshape(8, 16, WIDTH)
    send_plane(lambda n: dps.at[n], dpr, cs_sem, cr_sem)

    for zz in range(8):
        part = rcv2.at[pl.ds(zz * 8, 8)]
        pltpu.make_async_copy(part, part, br_sem.at[zz]).wait()
    sc[...] = rcv2[...].reshape(1024, 128).astype(F32)
    returned = jnp.concatenate(
        [sc[pl.ds(j, 128, stride=8), :].astype(BF) for j in range(8)], axis=1
    )
    three = jnp.dot(combine3, returned, preferred_element_type=F32)
    routed = three[0:16] + (three[16:32] + three[32:48])
    pltpu.make_async_copy(dpr, dpr, cr_sem).wait()
    dense = dpr[0].astype(F32)
    for i in range(1, 8):
        dense = dense + dpr[i].astype(F32)
    fin_s[...] = routed + switch * dense
    swap_f = pltpu.make_async_remote_copy(
        src_ref=fin_s, dst_ref=fin_r, send_sem=fs_sem, recv_sem=fr_sem,
        device_id=other, device_id_type=MESH,
    )
    swap_f.start()
    sent_all(snd, ms_sem, 64)
    sent_all(snd2, bs_sem, 64)
    sent_all(dtok, ts_sem, 8)
    sent_all(dps, cs_sem, 8)
    for cp in step1 + step2:
        cp.wait_send()
    for d in range(8):
        forward(d).wait_send()
    swap_f.wait()
    out[...] = (middle + (fin_s[...] + fin_r[...])).astype(BF)


def hand_over(a, b, c, a_out, b_out, c_out):
    a_out[...] = a[...]
    b_out[...] = b[...]
    c_out[...] = c[...]


def per_device(
    residual_in, lengths, cache_keys, cache_values, attend_gain, query_proj, key_proj,
    value_proj, lambdas, head_gain, out_proj, channel_gain, routes, route_weight,
    expert_gate, expert_up, expert_down, dense_gate, dense_up, dense_down, dense_mixer,
):
    inverse = np.float32(10000.0) ** (-np.arange(32, dtype=np.float32) / np.float32(32))
    frequency = jnp.asarray(np.tile(inverse, 4)[None, :])
    vm = pl.BlockSpec(memory_space=pltpu.VMEM)
    sm = pl.BlockSpec(memory_space=pltpu.SMEM)
    hb = pl.BlockSpec(memory_space=pl.ANY)
    DMA = pltpu.SemaphoreType.DMA
    V = pltpu.VMEM
    out, keys, values = pl.pallas_call(
        body,
        name="layer",
        out_shape=(
            jax.ShapeDtypeStruct((SEQS, WIDTH), BF),
            jax.ShapeDtypeStruct((SEQS, 128), BF),
            jax.ShapeDtypeStruct((SEQS, 128), BF),
        ),
        in_specs=[vm] * 6 + [sm] * 2 + [vm] * 2 + [hb] * 12,
        out_specs=(vm, vm, vm),
        scratch_shapes=[
            V((SEQS, LENGTH, 128), BF), V((SEQS, LENGTH, 128), BF),
            V((1024, 256), BF), V((1024, 128), BF), V((1024, 128), BF), V((256, 1024), BF),
            V((2, 1024, 256), BF), V((2, 1024, 256), BF), V((2, 256, 1024), BF),
            V((8, 2, 3, 16, 1024), BF),
            V((64, 128), F32), V((SEQS, 128), F32), V((SEQS, 128), F32),
            V((64, 128), F32),
            V((SEQS, WIDTH), BF), V((SEQS, WIDTH), BF), V((SEQS, WIDTH), BF),
            V((1024, 128), F32),
            V((64, 16, 128), BF), V((64, 16, 128), BF), V((64, 16, 128), BF), V((64, 16, 128), BF),
            V((8, 16, WIDTH), BF), V((8, 16, WIDTH), BF), V((8, 16, WIDTH), BF),
            V((SEQS, WIDTH), F32), V((SEQS, WIDTH), F32),
            DMA((7,)), DMA((16,)), DMA((16,)), DMA((3,)),
            DMA((8,)), DMA((8,)), DMA((8,)), DMA((8,)), DMA((3,)), DMA((3,)),
            DMA, DMA, DMA, DMA((8,)), DMA, DMA, DMA, DMA((8,)), DMA, DMA,
            DMA, DMA, pltpu.SemaphoreType.REGULAR,
        ],
        compiler_params=pltpu.CompilerParams(
            collective_id=0, has_side_effects=True, vmem_limit_bytes=60 * 1024 * 1024
        ),
    )(
        residual_in, attend_gain, channel_gain, dense_mixer, head_gain, frequency,
        lengths, lambdas, routes.T, route_weight.T,
        cache_keys.reshape(SEQS, LENGTH, 128), cache_values.reshape(SEQS, LENGTH, 128),
        query_proj, key_proj, value_proj, out_proj,
        expert_gate[0], expert_up[0], expert_down[0], dense_gate.T, dense_up.T, dense_down,
    )
    out, keys, values = pl.pallas_call(
        hand_over,
        name="hand_over",
        out_shape=(
            jax.ShapeDtypeStruct((SEQS, WIDTH), BF),
            jax.ShapeDtypeStruct((SEQS, 128), BF),
            jax.ShapeDtypeStruct((SEQS, 128), BF),
        ),
        in_specs=[vm] * 3,
        out_specs=(vm, vm, vm),
    )(out, keys, values)
    return out, keys.reshape(SEQS, 1, 128), values.reshape(SEQS, 1, 128)


def solution(mesh):
    placed = (
        P("ep", None), P("ep"), P("ep", "tp", None, None), P("ep", "tp", None, None), P(),
        P(None, "tp"), P(None, "tp"), P(None, "tp"), P("tp"), P(), P("tp", None), P(),
        P("ep", None), P("ep", None), P("ep", None, "tp"), P("ep", None, "tp"),
        P("ep", "tp", None), P(None, ("ep", "tp")), P(None, ("ep", "tp")),
        P(("ep", "tp"), None), P(),
    )
    return jax.shard_map(
        per_device, mesh=mesh, in_specs=placed,
        out_specs=(P("ep", None), P("ep", "tp", None), P("ep", "tp", None)),
        check_vma=False,
    )
```

time: 62.2 us -> 44.4 us (0.71)
  local copies, waits for them, and re-layouts: 10.5 us -> 0 us
  Pallas kernels: 49.2 us -> 43.5 us
  other arithmetic: 1.47 us -> 0 us
    pallas_call x1, Pallas kernels: 49.2 us -> 42.1 us  [per_device(): pl.pallas_call(body, name='layer', out_shape=(jax.ShapeDtypeStruct((SEQS,...]
    unnamed x5 -> x0, local copies, waits for them, and re-layouts: 6.64 us -> none
    reshape x3 -> x0, local copies, waits for them, and re-layouts: 3.83 us -> none  [the longest x1 1.28 us: per_device(): attend_gain.reshape(1, -1)]
    pallas_call x0 -> x1, Pallas kernels: none -> 1.39 us  [per_device(): pl.pallas_call(hand_over, name='hand_over', out_shape=(jax.ShapeDtypeStru...]
    concatenate x1 -> x0, other arithmetic: 0.69 us -> none  [per_device(): cosine = jnp.concatenate([cos, cos, cos, cos], axis=1)]
    convert_element_type x1 -> x0, other arithmetic: 0.66 us -> none  [per_device(): angles = lengths.astype(F32)[:, None] * inverse]
where the time goes in v2:
time: 44.4 us; the launch traced here: 44.2 us
  Pallas kernels  43.5 us (98%)
  between operations  0.65 us (1%)
    pallas_call x1, Pallas kernels, per_device(): pl.pallas_call(body, name='layer', out_shape=(jax.ShapeDtypeStruct((SEQS,...  42.1 us
    pallas_call x1, Pallas kernels, per_device(): pl.pallas_call(hand_over, name='hand_over', out_shape=(jax.ShapeDtypeStru...  1.39 us

profile of v2, /device:TPU:1, one launch (start us, length us, event | category | flops | bytes accessed | tf_op | source)
XLA Modules:
  0.0 44.2 jit_solution(2312943281912410017)
XLA Ops:
  0.6 42.1 %layer.1 = (bf16[16,1024]{1,0:T(8,128)(2,1)}, bf16[16,128]{1,0:T(8,128)(2,1)}, bf16[16,128]{1,0:T(8,128)(2,1)}) custom-call(bf16[16,1024]{1,0:T(8,128)(2,1)} %residual.1, bf16[1024]{0:T(1024)(128)(2,1)} %attend_gain.1, bf16[1024]{0:T(1024)(128)(2,1)} %channel_gain.1, bf16[1024]{0:T(1024)(128)(2,1)} %mixer.1, bf16[128]{0:T(256)(128)(2,1)} %head_gain.1, ...), custom_call_target="tpu_custom_call" | custom-call | tf_op jit(solution)/shard_map/layer/pallas_call | solution.py:441
  42.8 1.4 %hand_over.1 = (bf16[16,1024]{1,0:T(8,128)(2,1)}, bf16[16,128]{1,0:T(8,128)(2,1)}, bf16[16,128]{1,0:T(8,128)(2,1)}) custom-call(bf16[16,1024]{1,0:T(8,128)(2,1)} %get-tuple-element.9.a, bf16[16,128]{1,0:T(8,128)(2,1)} %get-tuple-element.10.b, bf16[16,128]{1,0:T(8,128)(2,1)} %get-tuple-element.11.c), custom_call_target="tpu_custom_call" | custom-call | tf_op jit(solution)/shard_map/hand_over/pallas_call | solution.py:478

commit v3 on v2

--- a/solution.py
+++ b/solution.py
@@ -24,11 +24,13 @@
 
 
 def body(
-    residual, attend_gain, channel_gain, mixer, head_gain, frequency,
-    lengths, lambdas, routes_turned, weight_turned,
+    residual_h, attend_gain_h, channel_gain_h, mixer_h, head_gain_h, frequency_h,
+    lengths_h, lambdas_h, routes_h, weights_h,
     cache_keys, cache_values, w_query, w_key, w_value, w_out,
     e_gate, e_up, e_down, d_gate, d_up, d_down,
-    out, new_keys, new_values,
+    out_h, new_keys_h, new_values_h,
+    residual, attend_gain, channel_gain, mixer, head_gain, frequency,
+    lengths, lambdas, routes_turned, weight_turned, out, new_keys, new_values, in_sem, out_sem,
     kbuf, vbuf, wq, wk, wv, wo, egb, eub, edb, dwb,
     qs, kn, nv, att, pa, pb, nsb, sc, snd, rcv, snd2, rcv2, dtok, dps, dpr, fin_s, fin_r,
     load_sem, k_sem, v_sem, own_sem, zs_sem, zr_sem, ps_sem, pr_sem, es_sem, er_sem,
@@ -40,17 +42,27 @@
     z = ep // 16
     y = (ep // 4) % 4
     x = ep % 4
-    parity = x % 2
-    me = z * 8 + y * 2 + x // 2
-    self_in = parity == c
     other = (ep, 1 - c)
-
+    selfish = c == 0
+
+    def chip(dz, dy, dx):
+        return ((z + dz + NZ) % NZ) * 16 + ((y + dy) % 4) * 4 + (x + dx) % 4
+
+    partners = []
+    for p, dz in ((0, 0), (1, -1), (2, 1)):
+        for dy in (2, 1, 3, 0):
+            for dx in (2, 1, 3, 0):
+                back = ((3 - p) % 3) * 16 + ((4 - dy) % 4) * 4 + (4 - dx) % 4
+                partners.append((chip(4 * c + dz, dy, dx), p * 16 + dy * 4 + dx, back))
+    for h in range(2):
+        for dy in (2, 1, 3, 0):
+            for j in range(2):
+                back = 48 + (1 - h) * 8 + ((4 - dy) % 4) * 2 + (c + j) % 2
+                partners.append((chip(2 + 4 * h, dy, c + 2 * j), 48 + h * 8 + dy * 2 + j, back))
     plane = []
-    for k in range(8):
-        yy = (y + 3 - k // 2) % 4
-        xh = (x // 2 + 1 - k % 2) % 2
-        plane.append((yy * 4 + xh * 2 + c, yy * 2 + xh))
-    mine = me % 8
+    for dy in (2, 1, 3, 0):
+        for j in range(2):
+            plane.append((chip(0, dy, c + 2 * j), dy * 2 + j, ((4 - dy) % 4) * 2 + (c + j) % 2))
 
     def z_peer(d):
         return (((z + d) % NZ) * 16 + y * 4 + x, c)
@@ -66,73 +78,49 @@
         pltpu.make_async_copy(src, dwb.at[z, c, i], own_sem.at[i])
         for i, src in enumerate([d_gate, d_up, d_down])
     ]
-    kv = [
-        (
-            pltpu.make_async_copy(cache_keys.at[s], kbuf.at[s], k_sem.at[s]),
-            pltpu.make_async_copy(cache_values.at[s], vbuf.at[s], v_sem.at[s]),
-        )
-        for s in range(SEQS)
+    kv = []
+    for quarter in range(4):
+        part = pl.ds(4 * quarter, 4)
+        kv.append(
+            (
+                pltpu.make_async_copy(cache_keys.at[part], kbuf.at[part], k_sem.at[quarter]),
+                pltpu.make_async_copy(cache_values.at[part], vbuf.at[part], v_sem.at[quarter]),
+            )
+        )
+    small = [
+        pltpu.make_async_copy(src, dst, in_sem.at[i])
+        for i, (src, dst) in enumerate(
+            [(residual_h, residual), (attend_gain_h, attend_gain), (frequency_h, frequency),
+             (lengths_h, lengths), (lambdas_h, lambdas), (routes_h, routes_turned),
+             (weights_h, weight_turned), (channel_gain_h, channel_gain), (mixer_h, mixer),
+             (head_gain_h, head_gain)]
+        )
     ]
-    for cp in own_parts:
+    for cp in own_parts + small[:5]:
         cp.start()
     for i in range(3):
         loads[i].start()
 
-    def stream(sequences):
-        for kind in range(2):
-            for s in sequences:
-                kv[s][kind].start()
-
-    stream(range(8))
-
+    kv[0][0].start()
+    kv[0][1].start()
+    for kind in range(2):
+        for quarter in (1, 2, 3):
+            kv[quarter][kind].start()
     barrier = pltpu.get_barrier_semaphore()
     for d in (4, 3, 5, 2, 6, 1, 7):
         pl.semaphore_signal(barrier, inc=1, device_id=z_peer(d), device_id_type=MESH)
-    for chip, slot in plane:
-
-        @pl.when(jnp.logical_not(jnp.logical_and(self_in, slot == mine)))
-        def _(chip=chip):
-            pl.semaphore_signal(barrier, inc=1, device_id=(z * 16 + chip, parity), device_id_type=MESH)
-
+    for k in range(15, 0, -1):
+        pl.semaphore_signal(
+            barrier, inc=1, device_id=(chip(0, k // 4, k % 4), c), device_id_type=MESH
+        )
     pl.semaphore_signal(barrier, inc=1, device_id=other, device_id_type=MESH)
 
-    row128 = lax.broadcasted_iota(jnp.int32, (128, SEQS), 0)
-    expert_t = (row128 // 2) * 2 + c
-    hit_t = jnp.zeros((128, SEQS), F32)
-    weight_t = jnp.zeros((128, SEQS), F32)
-    for k in range(6):
-        same = routes_turned[k : k + 1, :] == expert_t
-        hit_t = hit_t + jnp.where(same, 1.0, 0.0)
-        weight_t = weight_t + jnp.where(same, weight_turned[k : k + 1, :], 0.0)
-    up_tri = jnp.where(
-        lax.broadcasted_iota(jnp.int32, (SEQS, SEQS), 0)
-        < lax.broadcasted_iota(jnp.int32, (SEQS, SEQS), 1),
-        1.0, 0.0,
-    )
-    rank_t = jnp.dot(hit_t.astype(BF), up_tri.astype(BF), preferred_element_type=F32)
-    pick_t = jnp.where(rank_t == (row128 % 2).astype(F32), hit_t, 0.0).astype(BF)
-
-    combine_t = jnp.where(rank_t == (row128 % 2).astype(F32), weight_t, 0.0)
-    c_hi = combine_t.astype(BF)
-    rest = combine_t - c_hi.astype(F32)
-    c_mid = rest.astype(BF)
-    c_lo = (rest - c_mid.astype(F32)).astype(BF)
-    eye = jnp.where(
-        lax.broadcasted_iota(jnp.int32, (SEQS, SEQS), 0)
-        == lax.broadcasted_iota(jnp.int32, (SEQS, SEQS), 1),
-        1.0, 0.0,
-    ).astype(BF)
-    combine3 = jnp.concatenate(
-        [
-            lax.dot_general(eye, part, (((1,), (1,)), ((), ())), preferred_element_type=F32)
-            for part in (c_hi, c_mid, c_lo)
-        ],
-        axis=0,
-    ).astype(BF)
-
-    stream(range(8, SEQS))
+    for cp in small[5:]:
+        cp.start()
     loads[3].start()
 
+    for cp in small[:5]:
+        cp.wait()
     res = residual[...].astype(F32)
     normed = norm(res, attend_gain[...].astype(F32).reshape(1, WIDTH)).astype(BF)
     for i in range(3):
@@ -157,6 +145,12 @@
     k_rot = rotated(kk)
     new_keys[...] = k_rot
     new_values[...] = vv
+    results = [
+        pltpu.make_async_copy(new_keys, new_keys_h, out_sem.at[0]),
+        pltpu.make_async_copy(new_values, new_values_h, out_sem.at[1]),
+    ]
+    for cp in results:
+        cp.start()
     kn[...] = k_rot.astype(F32)
     nv[...] = vv.astype(F32)
     for g in range(2):
@@ -164,7 +158,7 @@
         qs[pl.ds(g, SEQS, stride=4), :] = jnp.where(lane128 < 64, q_rot, 0.0)
         qs[pl.ds(2 + g, SEQS, stride=4), :] = jnp.where(lane128 < 64, 0.0, q_rot)
 
-    pl.semaphore_wait(barrier, 7 + 8 + 1 - self_in.astype(jnp.int32))
+    pl.semaphore_wait(barrier, 7 + 15 + 1)
     for d in (4, 3, 5, 2, 6, 1, 7):
         pl.semaphore_signal(line_sem, inc=1, device_id=z_peer(d), device_id_type=MESH)
 
@@ -207,9 +201,8 @@
     turned = (((1,), (1,)), ((), ()))
 
     def attend(pairs):
-        for p in pairs:
-            kv[2 * p][0].wait()
-            kv[2 * p + 1][0].wait()
+        for quarter in sorted({p // 2 for p in pairs}):
+            kv[quarter][0].wait()
         scores, own = [], []
         for p in pairs:
             query = qs[8 * p : 8 * p + 8, :]
@@ -234,9 +227,8 @@
             own_weights.append(
                 (share_own - lam * pltpu.roll(share_own, 6, 0)).astype(BF).astype(F32)
             )
-        for p in pairs:
-            kv[2 * p][1].wait()
-            kv[2 * p + 1][1].wait()
+        for quarter in sorted({p // 2 for p in pairs}):
+            kv[quarter][1].wait()
         for i, p in enumerate(pairs):
             first_a = jnp.dot(weights[i], vbuf[2 * p], preferred_element_type=F32)
             second_a = jnp.dot(weights[i], vbuf[2 * p + 1], preferred_element_type=F32)
@@ -245,12 +237,15 @@
                 jnp.where(low8, first_a, second_a) + own_weights[i] * value
             )
 
-    attend((0, 1, 2, 3))
+    attend((0, 1))
+
+    attend((2, 3, 4, 5, 6, 7))
+
     for i in range(4, 7):
         loads[i].start()
 
-    attend((4, 5, 6, 7))
-
+    for cp in small[5:]:
+        cp.wait()
     gain_h = head_gain[...].astype(F32).reshape(1, 128)
     rows = jnp.concatenate(
         [(norm(att[pl.ds(g, SEQS, stride=4), :], gain_h) * 0.8).astype(BF) for g in range(2)], axis=1
@@ -264,6 +259,47 @@
     swap_a.start()
     for cp in swaps:
         cp.start()
+
+    row128 = lax.broadcasted_iota(jnp.int32, (128, SEQS), 0)
+    block = row128 // 2
+    in_half = block >= 48
+    third = block // 16
+    dz_t = jnp.where(in_half, 2 + 4 * ((block // 8) % 2), 4 * c + jnp.where(third == 2, 1, -third))
+    dy_t = jnp.where(in_half, (block // 2) % 4, (block // 4) % 4)
+    dx_t = jnp.where(in_half, c + 2 * (block % 2), block % 4)
+    expert_t = ((z + dz_t + NZ) % NZ) * 16 + ((y + dy_t) % 4) * 4 + (x + dx_t) % 4
+    hit_t = jnp.zeros((128, SEQS), F32)
+    weight_t = jnp.zeros((128, SEQS), F32)
+    for k in range(6):
+        same = routes_turned[k : k + 1, :] == expert_t
+        hit_t = hit_t + jnp.where(same, 1.0, 0.0)
+        weight_t = weight_t + jnp.where(same, weight_turned[k : k + 1, :], 0.0)
+    up_tri = jnp.where(
+        lax.broadcasted_iota(jnp.int32, (SEQS, SEQS), 0)
+        < lax.broadcasted_iota(jnp.int32, (SEQS, SEQS), 1),
+        1.0, 0.0,
+    )
+    rank_t = jnp.dot(hit_t.astype(BF), up_tri.astype(BF), preferred_element_type=F32)
+    pick_t = jnp.where(rank_t == (row128 % 2).astype(F32), hit_t, 0.0).astype(BF)
+
+    combine_t = jnp.where(rank_t == (row128 % 2).astype(F32), weight_t, 0.0)
+    c_hi = combine_t.astype(BF)
+    rest = combine_t - c_hi.astype(F32)
+    c_mid = rest.astype(BF)
+    c_lo = (rest - c_mid.astype(F32)).astype(BF)
+    eye = jnp.where(
+        lax.broadcasted_iota(jnp.int32, (SEQS, SEQS), 0)
+        == lax.broadcasted_iota(jnp.int32, (SEQS, SEQS), 1),
+        1.0, 0.0,
+    ).astype(BF)
+    combine3 = jnp.concatenate(
+        [
+            lax.dot_general(eye, part, (((1,), (1,)), ((), ())), preferred_element_type=F32)
+            for part in (c_hi, c_mid, c_lo)
+        ],
+        axis=0,
+    ).astype(BF)
+
     swap_a.wait()
     middle = (res + (pa[...].astype(F32) + pb[...].astype(F32))).astype(BF).astype(F32)
     ns = norm(middle, channel_gain[...].astype(F32).reshape(1, WIDTH)).astype(BF)
@@ -276,62 +312,41 @@
         for j in range(8):
             sc[pl.ds(j, 128, stride=8), :] = values[:, 128 * j : 128 * j + 128]
 
-    def send_blocks(src, dst, send_sem, recv_sem, distances):
-        for dz in distances:
-            zz = (z + dz) % NZ
-            for chip, slot in plane:
-                n = zz * 8 + slot
-                remote = pltpu.make_async_remote_copy(
-                    src_ref=src.at[n], dst_ref=dst.at[me], send_sem=send_sem,
-                    recv_sem=recv_sem.at[z], device_id=(zz * 16 + chip, parity),
-                    device_id_type=MESH,
-                )
-                if dz:
-                    remote.start()
-                    continue
-                self_block = jnp.logical_and(self_in, slot == mine)
-
-                @pl.when(self_block)
-                def _(n=n):
-                    pltpu.make_async_copy(src.at[n], dst.at[me], recv_sem.at[z]).start()
-
-                @pl.when(jnp.logical_not(self_block))
-                def _(remote=remote):
-                    remote.start()
+    def send_each(peers, pick_src, dst, send_sem, recv_sem):
+        for target, here, there in peers:
+            remote = pltpu.make_async_remote_copy(
+                src_ref=pick_src(here), dst_ref=dst.at[there], send_sem=send_sem,
+                recv_sem=recv_sem, device_id=(target, c), device_id_type=MESH,
+            )
+            if here:
+                remote.start()
+                continue
+
+            @pl.when(selfish)
+            def _():
+                pltpu.make_async_copy(pick_src(0), dst.at[0], recv_sem).start()
+
+            @pl.when(jnp.logical_not(selfish))
+            def _(remote=remote):
+                remote.start()
 
     def sent_all(buf, send_sem, count):
-        @pl.when(self_in)
+        @pl.when(selfish)
         def _():
             part = buf.at[pl.ds(0, count - 1)]
             pltpu.make_async_copy(part, part, send_sem).wait()
 
-        @pl.when(jnp.logical_not(self_in))
+        @pl.when(jnp.logical_not(selfish))
         def _():
             pltpu.make_async_copy(buf, buf, send_sem).wait()
-
-    def send_plane(pick_src, dst, send_sem, recv_sem):
-        for chip, slot in plane:
-            src = pick_src(slot)
-            self_block = jnp.logical_and(self_in, slot == mine)
-
-            @pl.when(self_block)
-            def _(src=src):
-                pltpu.make_async_copy(src, dst.at[mine], recv_sem).start()
-
-            @pl.when(jnp.logical_not(self_block))
-            def _(src=src, chip=chip):
-                pltpu.make_async_remote_copy(
-                    src_ref=src, dst_ref=dst.at[mine], send_sem=send_sem,
-                    recv_sem=recv_sem, device_id=(z * 16 + chip, parity), device_id_type=MESH,
-                ).start()
 
     picked = jnp.dot(pick_t, ns, preferred_element_type=F32)
     for j in range(8):
         sc[pl.ds(j, 128, stride=8), :] = picked[:, 128 * j : 128 * j + 128]
     snd[...] = sc[...].reshape(64, 16, 128).astype(BF)
     pl.semaphore_wait(line_sem, 7)
-    send_blocks(snd, rcv, ms_sem, mr_sem, (4, 3, 5, 2, 6, 1, 7, 0))
-    send_plane(lambda n: nsb, dtok, ts_sem, tr_sem)
+    send_each(partners, lambda n: snd.at[n], rcv, ms_sem, mr_sem)
+    send_each(plane, lambda n: nsb, dtok, ts_sem, tr_sem)
 
     for d in (7, 1, 4):
         z_wait(d)
@@ -346,31 +361,22 @@
     for cp in swaps:
         cp.wait()
 
-    def serve(distances):
-        count = len(distances)
-        slots = [pl.ds(((z + d) % NZ) * 8, 8) for d in distances]
-        for d, part in zip(distances, slots):
-            ref = rcv.at[part]
-            pltpu.make_async_copy(ref, ref, mr_sem.at[(z + d) % NZ]).wait()
-        for i, part in enumerate(slots):
-            sc[128 * i : 128 * i + 128, :] = rcv[part].reshape(128, 128).astype(F32)
-        rows = jnp.concatenate(
-            [sc[pl.ds(j, 16 * count, stride=8), :].astype(BF) for j in range(8)], axis=1
-        )
-        total = None
-        for h in range(2):
-            gate = jnp.dot(rows, egb[h], preferred_element_type=F32)
-            upper = jnp.dot(rows, eub[h], preferred_element_type=F32)
-            hidden = (silu(gate) * upper).astype(BF)
-            half = jnp.dot(hidden, edb[h], preferred_element_type=F32).astype(BF).astype(F32)
-            total = half if total is None else total + half
-        for j in range(8):
-            sc[pl.ds(j, 16 * count, stride=8), :] = total[:, 128 * j : 128 * j + 128]
-        for i, part in enumerate(slots):
-            snd2[part] = sc[128 * i : 128 * i + 128, :].reshape(8, 16, 128).astype(BF)
-        send_blocks(snd2, rcv2, bs_sem, br_sem, distances)
-
-    serve((4, 3, 5, 2, 6, 1, 7, 0))
+    pltpu.make_async_copy(rcv, rcv, mr_sem).wait()
+    sc[...] = rcv[...].reshape(1024, 128).astype(F32)
+    rows = jnp.concatenate(
+        [sc[pl.ds(j, 128, stride=8), :].astype(BF) for j in range(8)], axis=1
+    )
+    total = None
+    for h in range(2):
+        gate = jnp.dot(rows, egb[h], preferred_element_type=F32)
+        upper = jnp.dot(rows, eub[h], preferred_element_type=F32)
+        hidden = (silu(gate) * upper).astype(BF)
+        half = jnp.dot(hidden, edb[h], preferred_element_type=F32).astype(BF).astype(F32)
+        total = half if total is None else total + half
+    for j in range(8):
+        sc[pl.ds(j, 128, stride=8), :] = total[:, 128 * j : 128 * j + 128]
+    snd2[...] = sc[...].reshape(64, 16, 128).astype(BF)
+    send_each(partners, lambda n: snd2.at[n], rcv2, bs_sem, br_sem)
 
     for d in (2, 6, 3, 5):
         z_wait(d)
@@ -387,11 +393,9 @@
     upper = lax.dot_general(xd, up_w, turned, preferred_element_type=F32)
     hidden = (silu(gate) * upper).astype(BF)
     dps[...] = jnp.dot(hidden, down_w, preferred_element_type=F32).astype(BF).reshape(8, 16, WIDTH)
-    send_plane(lambda n: dps.at[n], dpr, cs_sem, cr_sem)
-
-    for zz in range(8):
-        part = rcv2.at[pl.ds(zz * 8, 8)]
-        pltpu.make_async_copy(part, part, br_sem.at[zz]).wait()
+    send_each(plane, lambda n: dps.at[n], dpr, cs_sem, cr_sem)
+
+    pltpu.make_async_copy(rcv2, rcv2, br_sem).wait()
     sc[...] = rcv2[...].reshape(1024, 128).astype(F32)
     returned = jnp.concatenate(
         [sc[pl.ds(j, 128, stride=8), :].astype(BF) for j in range(8)], axis=1
@@ -418,6 +422,10 @@
         forward(d).wait_send()
     swap_f.wait()
     out[...] = (middle + (fin_s[...] + fin_r[...])).astype(BF)
+    last = pltpu.make_async_copy(out, out_h, out_sem.at[2])
+    last.start()
+    for cp in results + [last]:
+        cp.wait()
 
 
 def hand_over(a, b, c, a_out, b_out, c_out):
@@ -434,7 +442,6 @@
     inverse = np.float32(10000.0) ** (-np.arange(32, dtype=np.float32) / np.float32(32))
     frequency = jnp.asarray(np.tile(inverse, 4)[None, :])
     vm = pl.BlockSpec(memory_space=pltpu.VMEM)
-    sm = pl.BlockSpec(memory_space=pltpu.SMEM)
     hb = pl.BlockSpec(memory_space=pl.ANY)
     DMA = pltpu.SemaphoreType.DMA
     V = pltpu.VMEM
@@ -446,9 +453,13 @@
             jax.ShapeDtypeStruct((SEQS, 128), BF),
             jax.ShapeDtypeStruct((SEQS, 128), BF),
         ),
-        in_specs=[vm] * 6 + [sm] * 2 + [vm] * 2 + [hb] * 12,
-        out_specs=(vm, vm, vm),
+        in_specs=[hb] * 22,
+        out_specs=(hb, hb, hb),
         scratch_shapes=[
+            V((SEQS, WIDTH), BF), V((WIDTH,), BF), V((WIDTH,), BF), V((WIDTH,), BF),
+            V((128,), BF), V((1, 128), F32), pltpu.SMEM((SEQS,), jnp.int32),
+            pltpu.SMEM((2,), F32), V((6, SEQS), jnp.int32), V((6, SEQS), F32),
+            V((SEQS, WIDTH), BF), V((SEQS, 128), BF), V((SEQS, 128), BF), DMA((10,)), DMA((3,)),
             V((SEQS, LENGTH, 128), BF), V((SEQS, LENGTH, 128), BF),
             V((1024, 256), BF), V((1024, 128), BF), V((1024, 128), BF), V((256, 1024), BF),
             V((2, 1024, 256), BF), V((2, 1024, 256), BF), V((2, 256, 1024), BF),
@@ -460,9 +471,9 @@
             V((64, 16, 128), BF), V((64, 16, 128), BF), V((64, 16, 128), BF), V((64, 16, 128), BF),
             V((8, 16, WIDTH), BF), V((8, 16, WIDTH), BF), V((8, 16, WIDTH), BF),
             V((SEQS, WIDTH), F32), V((SEQS, WIDTH), F32),
-            DMA((7,)), DMA((16,)), DMA((16,)), DMA((3,)),
+            DMA((7,)), DMA((4,)), DMA((4,)), DMA((3,)),
             DMA((8,)), DMA((8,)), DMA((8,)), DMA((8,)), DMA((3,)), DMA((3,)),
-            DMA, DMA, DMA, DMA((8,)), DMA, DMA, DMA, DMA((8,)), DMA, DMA,
+            DMA, DMA, DMA, DMA, DMA, DMA, DMA, DMA, DMA, DMA,
             DMA, DMA, pltpu.SemaphoreType.REGULAR,
         ],
         compiler_params=pltpu.CompilerParams(

time: 44.4 us -> 43 us (0.968)
  Pallas kernels: 43.5 us -> 42.2 us
    pallas_call x1, Pallas kernels: 42.1 us -> 40.8 us  [per_device(): pl.pallas_call(body, name='layer', out_shape=(jax.ShapeDtypeStruct((SEQS,...]
where the time goes in v3:
time: 43 us; the launch traced here: 42.8 us
  Pallas kernels  42.2 us (98%)
  between operations  0.65 us (2%)
    pallas_call x1, Pallas kernels, per_device(): pl.pallas_call(body, name='layer', out_shape=(jax.ShapeDtypeStruct((SEQS,...  40.8 us
    pallas_call x1, Pallas kernels, per_device(): pl.pallas_call(hand_over, name='hand_over', out_shape=(jax.ShapeDtypeStru...  1.39 us

profile of v3, /device:TPU:1, one launch (start us, length us, event | category | flops | bytes accessed | tf_op | source)
XLA Modules:
  0.0 42.8 jit_solution(6854092496150923447)
XLA Ops:
  0.6 40.8 %layer.1 = (bf16[16,1024]{1,0:T(8,128)(2,1)}, bf16[16,128]{1,0:T(8,128)(2,1)}, bf16[16,128]{1,0:T(8,128)(2,1)}) custom-call(bf16[16,1024]{1,0:T(8,128)(2,1)} %residual_h.1, bf16[1024]{0:T(1024)(128)(2,1)} %attend_gain_h.1, bf16[1024]{0:T(1024)(128)(2,1)} %channel_gain_h.1, bf16[1024]{0:T(1024)(128)(2,1)} %mixer_h.1, bf16[128]{0:T(256)(128)(2,1)} %head_gain_h.1, ...), custom_call_target="tpu_custom_call" | custom-call | tf_op jit(solution)/shard_map/layer/pallas_call | solution.py:448
  41.4 1.4 %hand_over.1 = (bf16[16,1024]{1,0:T(8,128)(2,1)}, bf16[16,128]{1,0:T(8,128)(2,1)}, bf16[16,128]{1,0:T(8,128)(2,1)}) custom-call(bf16[16,1024]{1,0:T(8,128)(2,1)} %get-tuple-element.9.a, bf16[16,128]{1,0:T(8,128)(2,1)} %get-tuple-element.10.b, bf16[16,128]{1,0:T(8,128)(2,1)} %get-tuple-element.11.c), custom_call_target="tpu_custom_call" | custom-call | tf_op jit(solution)/shard_map/hand_over/pallas_call | solution.py:489

commit v4 on v3

--- a/solution.py
+++ b/solution.py
@@ -101,11 +101,6 @@
     for i in range(3):
         loads[i].start()
 
-    kv[0][0].start()
-    kv[0][1].start()
-    for kind in range(2):
-        for quarter in (1, 2, 3):
-            kv[quarter][kind].start()
     barrier = pltpu.get_barrier_semaphore()
     for d in (4, 3, 5, 2, 6, 1, 7):
         pl.semaphore_signal(barrier, inc=1, device_id=z_peer(d), device_id_type=MESH)
@@ -115,6 +110,9 @@
         )
     pl.semaphore_signal(barrier, inc=1, device_id=other, device_id_type=MESH)
 
+    for keys, values in kv:
+        keys.start()
+        values.start()
     for cp in small[5:]:
         cp.start()
     loads[3].start()
@@ -162,16 +160,26 @@
     for d in (4, 3, 5, 2, 6, 1, 7):
         pl.semaphore_signal(line_sem, inc=1, device_id=z_peer(d), device_id_type=MESH)
 
-    def z_copy(d, hop):
-        ref = dwb.at[(z + hop + d) % NZ, c]
-        return pltpu.make_async_remote_copy(
-            src_ref=ref, dst_ref=ref, send_sem=zs_sem.at[d], recv_sem=zr_sem.at[d],
+    moved = []
+
+    def z_send(d, hop, part):
+        ref = dwb.at[(z + hop + d) % NZ, c, part]
+        copy = pltpu.make_async_remote_copy(
+            src_ref=ref, dst_ref=ref, send_sem=zs_sem.at[d, part], recv_sem=zr_sem.at[d, part],
             device_id=z_peer(hop), device_id_type=MESH,
         )
-
-    def z_wait(d):
-        ref = dwb.at[(z + d) % NZ, c]
-        pltpu.make_async_copy(ref, ref, zr_sem.at[d % NZ]).wait()
+        copy.start()
+        moved.append(copy)
+
+    def z_wait(d, part):
+        ref = dwb.at[(z + d) % NZ, c, part]
+        pltpu.make_async_copy(ref, ref, zr_sem.at[d, part]).wait()
+
+    def relay(part):
+        z_wait(7, part)
+        z_wait(1, part)
+        z_send(6, 1, part)
+        z_send(2, -1, part)
 
     def forward(d):
         ref = dwb.at[(z + d) % NZ, c]
@@ -182,9 +190,11 @@
 
     for cp in own_parts:
         cp.wait()
-    step1 = [z_copy(4, 4), z_copy(7, 1), z_copy(1, -1)]
-    for cp in step1:
-        cp.start()
+    for part in range(3):
+        z_send(7, 1, part)
+        z_send(1, -1, part)
+    z_send(6, 2, 0)
+    z_send(2, -2, 0)
     swaps = [
         pltpu.make_async_remote_copy(
             src_ref=src, dst_ref=dst.at[c], send_sem=es_sem.at[i], recv_sem=er_sem.at[i],
@@ -239,7 +249,8 @@
 
     attend((0, 1))
 
-    attend((2, 3, 4, 5, 6, 7))
+    attend((2, 3))
+    attend((4, 5, 6, 7))
 
     for i in range(4, 7):
         loads[i].start()
@@ -260,6 +271,7 @@
     for cp in swaps:
         cp.start()
 
+    relay(1)
     row128 = lax.broadcasted_iota(jnp.int32, (128, SEQS), 0)
     block = row128 // 2
     in_half = block >= 48
@@ -301,6 +313,7 @@
     ).astype(BF)
 
     swap_a.wait()
+    relay(2)
     middle = (res + (pa[...].astype(F32) + pb[...].astype(F32))).astype(BF).astype(F32)
     ns = norm(middle, channel_gain[...].astype(F32).reshape(1, WIDTH)).astype(BF)
     nsb[...] = ns
@@ -348,13 +361,19 @@
     send_each(partners, lambda n: snd.at[n], rcv, ms_sem, mr_sem)
     send_each(plane, lambda n: nsb, dtok, ts_sem, tr_sem)
 
-    for d in (7, 1, 4):
-        z_wait(d)
-    step2 = [z_copy(6, 1), z_copy(2, -1), z_copy(3, 1), z_copy(5, -1)]
-    for cp in step2:
-        cp.start()
-    for d in (1, 7, 4):
-        forward(d).start()
+    z_wait(7, 0)
+    z_wait(1, 0)
+    forward(7).start()
+    forward(1).start()
+    for part in range(3):
+        z_wait(6, part)
+        z_send(5, 1, part)
+        z_wait(2, part)
+        z_send(3, -1, part)
+    for part in range(3):
+        z_send(4, 2 - 4 * c, part)
+    forward(6).start()
+    forward(2).start()
 
     for i in range(4, 7):
         loads[i].wait()
@@ -378,8 +397,9 @@
     snd2[...] = sc[...].reshape(64, 16, 128).astype(BF)
     send_each(partners, lambda n: snd2.at[n], rcv2, bs_sem, br_sem)
 
-    for d in (2, 6, 3, 5):
-        z_wait(d)
+    for d in (3, 5, 4):
+        for part in range(3):
+            z_wait(d, part)
         forward(d).start()
     pltpu.make_async_copy(dtok, dtok, tr_sem).wait()
     for d in range(8):
@@ -416,7 +436,7 @@
     sent_all(snd2, bs_sem, 64)
     sent_all(dtok, ts_sem, 8)
     sent_all(dps, cs_sem, 8)
-    for cp in step1 + step2:
+    for cp in moved:
         cp.wait_send()
     for d in range(8):
         forward(d).wait_send()
@@ -472,7 +492,7 @@
             V((8, 16, WIDTH), BF), V((8, 16, WIDTH), BF), V((8, 16, WIDTH), BF),
             V((SEQS, WIDTH), F32), V((SEQS, WIDTH), F32),
             DMA((7,)), DMA((4,)), DMA((4,)), DMA((3,)),
-            DMA((8,)), DMA((8,)), DMA((8,)), DMA((8,)), DMA((3,)), DMA((3,)),
+            DMA((8, 3)), DMA((8, 3)), DMA((8,)), DMA((8,)), DMA((3,)), DMA((3,)),
             DMA, DMA, DMA, DMA, DMA, DMA, DMA, DMA, DMA, DMA,
             DMA, DMA, pltpu.SemaphoreType.REGULAR,
         ],

time: 43 us -> 41.8 us (0.972)
  Pallas kernels: 42.2 us -> 41 us
    pallas_call x1, Pallas kernels: 40.8 us -> 39.6 us  [per_device(): pl.pallas_call(body, name='layer', out_shape=(jax.ShapeDtypeStruct((SEQS,...]
where the time goes in v4:
time: 41.8 us; the launch traced here: 41.7 us
  Pallas kernels  41 us (98%)
  between operations  0.65 us (2%)
    pallas_call x1, Pallas kernels, per_device(): pl.pallas_call(body, name='layer', out_shape=(jax.ShapeDtypeStruct((SEQS,...  39.6 us
    pallas_call x1, Pallas kernels, per_device(): pl.pallas_call(hand_over, name='hand_over', out_shape=(jax.ShapeDtypeStru...  1.39 us

profile of v4, /device:TPU:1, one launch (start us, length us, event | category | flops | bytes accessed | tf_op | source)
XLA Modules:
  0.0 41.7 jit_solution(8534768423543048597)
XLA Ops:
  0.6 39.6 %layer.1 = (bf16[16,1024]{1,0:T(8,128)(2,1)}, bf16[16,128]{1,0:T(8,128)(2,1)}, bf16[16,128]{1,0:T(8,128)(2,1)}) custom-call(bf16[16,1024]{1,0:T(8,128)(2,1)} %residual_h.1, bf16[1024]{0:T(1024)(128)(2,1)} %attend_gain_h.1, bf16[1024]{0:T(1024)(128)(2,1)} %channel_gain_h.1, bf16[1024]{0:T(1024)(128)(2,1)} %mixer_h.1, bf16[128]{0:T(256)(128)(2,1)} %head_gain_h.1, ...), custom_call_target="tpu_custom_call" | custom-call | tf_op jit(solution)/shard_map/layer/pallas_call | solution.py:468
  40.3 1.4 %hand_over.1 = (bf16[16,1024]{1,0:T(8,128)(2,1)}, bf16[16,128]{1,0:T(8,128)(2,1)}, bf16[16,128]{1,0:T(8,128)(2,1)}) custom-call(bf16[16,1024]{1,0:T(8,128)(2,1)} %get-tuple-element.9.a, bf16[16,128]{1,0:T(8,128)(2,1)} %get-tuple-element.10.b, bf16[16,128]{1,0:T(8,128)(2,1)} %get-tuple-element.11.c), custom_call_target="tpu_custom_call" | custom-call | tf_op jit(solution)/shard_map/hand_over/pallas_call | solution.py:509
